TPU v7x, 256 devices: a whole 4x4x8 slice. The times are simulated.
256 devices in a mesh: sp: 64 (over z, x, core), tp: 4 (over y).
Axes of the slice: x: 4, y: 4, z: 8, core: 2. Of those that a mesh axis runs over, the one named last changes fastest.
Arguments:
- queries: bfloat16 [20480, 1024], P('sp', 'tp'), may hold values from -6.6 to 6.6
- key_matrix: bfloat16 [20480, 256], P('sp', 'tp'), may hold values from -6.6 to 6.6
- values: bfloat16 [20480, 256], P('sp', 'tp'), may hold values from -6 to 6
- query_gain: float32 [64], replicated, may hold values from 0.19 to 8
- key_norm_gain: float32 [64], replicated, may hold values from 0.19 to 8
- head_gain: float32 [1024], P('tp'), may hold values from 0.1 to 1.9
- out_proj: bfloat16 [1024, 2048], replicated, may hold values from -0.1875 to 0.1875
- residual: bfloat16 [20480, 2048], P('sp'), may hold values from -6 to 6
- ffn_gain: float32 [2048], replicated, may hold values from 0.1 to 1.9
- routes: int32 [20480, 4], P('sp'), may hold values from 0 to 255, all different within a row; in each aligned block of 320 rows (0 to 319, 320 to 639, ...) at most 10 rows name the same one
- route_weights: float32 [20480, 4], P('sp'), may hold values from 0.2 to 1
- expert_gate: bfloat16 [256, 2048, 512], P(('sp', 'tp')), may hold values from -0.125 to 0.125
- expert_up: bfloat16 [256, 2048, 512], P(('sp', 'tp')), may hold values from -0.125 to 0.125
- expert_down: bfloat16 [256, 512, 2048], P(('sp', 'tp')), may hold values from -0.25 to 0.25
- shared_gate: bfloat16 [2048, 512], P(None, 'tp'), may hold values from -0.125 to 0.125
- shared_up: bfloat16 [2048, 512], P(None, 'tp'), may hold values from -0.125 to 0.125
- shared_down: bfloat16 [512, 2048], P('tp'), may hold values from -0.25 to 0.25
Outputs:
- layer_out: bfloat16 [20480, 2048], P(('sp', 'tp'))
Inputs may be any that keep to these rules, and one draw needn't show every extreme that they name: `routes`: each row names 4 different experts; in each aligned block of 320 rows (the tokens of one index of sp) no expert is named more than 10 times, a bound that some block reaches.
All inputs are finite; a program needn't handle non-finite values.
Results may differ from a plain program's by a relative error of at most 0.019.
The roundings to bfloat16 on the way count: a program that leaves them out, or rounds other values in their place, can miss the bound.
Values may be sent and summed in bfloat16 or wider, within the bound.
A program may use at most 128 MiB of HBM per device.

v0:
```python
import jax
import jax.numpy as jnp
from jax import lax
from jax.sharding import PartitionSpec as P

HEAD_SIZE = 64
GRID_W = 64


EPS = 1e-06
THETA = 10000.0


def laid_out(tiles, dim):
    tiles = jnp.moveaxis(tiles, 0, dim)
    dims = tiles.shape
    return tiles.reshape(*dims[:dim], dims[dim] * dims[dim + 1], *dims[dim + 2 :])


def from_everyone(value, axis):
    length = lax.axis_size(axis)
    return lax.all_to_all(
        jnp.broadcast_to(value[None], (length, *value.shape)), axis, 0, 0, tiled=True
    )


def gather_directly(value, axis, dim):
    return laid_out(from_everyone(value, axis), dim)


def split_up(value, dim, length):
    dims = value.shape
    tiles = value.reshape(*dims[:dim], length, dims[dim] // length, *dims[dim + 1 :])
    return jnp.moveaxis(tiles, dim, 0)


def sent_and_summed(value, axis, dim):
    length = lax.axis_size(axis)
    tiles = lax.all_to_all(split_up(value, dim, length), axis, 0, 0, tiled=True)
    return jnp.sum(tiles.astype(jnp.float32), axis=0)


def final_norm(field, gain):
    mean_sq = jnp.mean(field * field, axis=-1, keepdims=True)
    return field * lax.rsqrt(mean_sq + EPS) * gain


def grid_tables(positions, sequence_total):
    grid_rows = sequence_total // GRID_W
    row_pos = (positions // GRID_W - grid_rows // 2).astype(jnp.float32)
    col_pos = (positions % GRID_W - GRID_W // 2).astype(jnp.float32)
    quarter = HEAD_SIZE // 4
    inverse = THETA ** (-jnp.arange(quarter, dtype=jnp.float32) / quarter)
    angles = jnp.concatenate([row_pos[:, None] * inverse, col_pos[:, None] * inverse], axis=1)
    return (jnp.cos(angles), jnp.sin(angles))


def apply_rotary(field, cosine_table, sine_table):
    row_count, head_count = (field.shape[0], field.shape[1])
    quarter = HEAD_SIZE // 4
    pieces = field.reshape(row_count, head_count, 2, 2, quarter)
    front_half = pieces[:, :, :, 0, :].reshape(row_count, head_count, 2 * quarter)
    back_half = pieces[:, :, :, 1, :].reshape(row_count, head_count, 2 * quarter)
    cos_wide = cosine_table[:, None, :]
    sin_wide = sine_table[:, None, :]
    new_front = (front_half * cos_wide - back_half * sin_wide).reshape(
        row_count, head_count, 2, 1, quarter
    )
    new_back = (front_half * sin_wide + back_half * cos_wide).reshape(
        row_count, head_count, 2, 1, quarter
    )
    return jnp.concatenate([new_front, new_back], axis=3).reshape(row_count, head_count, HEAD_SIZE)


def key_block_rows(piece_rows):
    return max((width for width in range(1, 2049) if piece_rows % width == 0))


def local(
    queries,
    key_matrix,
    values,
    query_gain,
    key_norm_gain,
    head_gain,
    out_proj,
    residual,
    ffn_gain,
    routes,
    route_weights,
    expert_gate,
    expert_up,
    expert_down,
    shared_gate,
    shared_up,
    shared_down,
):
    tok_count = queries.shape[0]
    head_count = queries.shape[1] // HEAD_SIZE
    sp_count = lax.axis_size("sp")
    tp_count = lax.axis_size("tp")
    tp_index = lax.axis_index("tp")
    sequence_total = tok_count * sp_count
    positions = lax.axis_index("sp") * tok_count + jnp.arange(tok_count, dtype=jnp.int32)
    cosine_table, sine_table = grid_tables(positions, sequence_total)
    rotated_query = apply_rotary(
        final_norm(
            queries.astype(jnp.float32).reshape(tok_count, head_count, HEAD_SIZE), query_gain
        ),
        cosine_table,
        sine_table,
    ).astype(jnp.bfloat16)
    rotated_key = (
        apply_rotary(
            final_norm(
                key_matrix.astype(jnp.float32).reshape(tok_count, 1, HEAD_SIZE), key_norm_gain
            ),
            cosine_table,
            sine_table,
        )
        .reshape(tok_count, HEAD_SIZE)
        .astype(jnp.bfloat16)
    )
    packed = jnp.concatenate([rotated_key, values], axis=1)
    query_rows = rotated_query.transpose(1, 0, 2).reshape(head_count * tok_count, HEAD_SIZE)
    score_scale = HEAD_SIZE ** (-0.5)
    start_state = (
        jnp.full((head_count * tok_count,), -1e30, jnp.float32),
        jnp.zeros((head_count * tok_count,), jnp.float32),
        jnp.zeros((head_count * tok_count, HEAD_SIZE), jnp.float32),
    )
    state = start_state
    piece = lax.all_gather(packed, "sp", axis=0, tiled=True)
    piece_rows = piece.shape[0]
    block_length = key_block_rows(piece_rows)
    key_blocks = piece.reshape(piece_rows // block_length, block_length, 2 * HEAD_SIZE)

    def step(carry, key_slab):
        run_max, run_total, run_acc = carry
        scores = (
            lax.dot_general(
                query_rows,
                key_slab[:, :HEAD_SIZE],
                (((1,), (1,)), ((), ())),
                preferred_element_type=jnp.float32,
            )
            * score_scale
        )
        new_max = jnp.maximum(run_max, jnp.max(scores, axis=1))
        factor = jnp.exp(run_max - new_max)
        expo_terms = jnp.exp(scores - new_max[:, None])
        new_total = run_total * factor + jnp.sum(expo_terms, axis=1)
        new_acc = run_acc * factor[:, None] + jnp.dot(
            expo_terms.astype(jnp.bfloat16),
            key_slab[:, HEAD_SIZE:],
            preferred_element_type=jnp.float32,
        )
        return ((new_max, new_total, new_acc), None)

    state, _ = lax.scan(step, state, key_blocks)
    run_max, run_total, run_acc = state
    attended = (
        (run_acc / run_total[:, None]).reshape(head_count, tok_count, HEAD_SIZE).transpose(1, 0, 2)
    )
    head_out = final_norm(attended, head_gain.reshape(head_count, HEAD_SIZE)).astype(jnp.bfloat16)
    head_out = head_out.reshape(tok_count, head_count * HEAD_SIZE)
    part_rows = tok_count // tp_count
    token_heads = lax.all_to_all(head_out, "tp", split_axis=0, concat_axis=1, tiled=True)
    own_resid = lax.dynamic_slice_in_dim(residual, tp_index * part_rows, part_rows, 0)
    hidden_own = (
        own_resid.astype(jnp.float32)
        + jnp.dot(token_heads, out_proj, preferred_element_type=jnp.float32)
    ).astype(jnp.bfloat16)
    normed_own = final_norm(hidden_own.astype(jnp.float32), ffn_gain).astype(jnp.bfloat16)
    normed = gather_directly(normed_own, "tp", 0)
    model_width = normed.shape[1]
    topk_count = routes.shape[1]
    capacity = max(2, 2 * tok_count * topk_count // (sp_count * tp_count))
    slot_total = sp_count * capacity
    flat_expert = routes.reshape(-1)
    entry_token = jnp.arange(tok_count * topk_count, dtype=jnp.int32) // topk_count
    is_mine = flat_expert % tp_count == tp_index
    target = flat_expert // tp_count
    onehot = (target[:, None] == jnp.arange(sp_count, dtype=jnp.int32)[None, :]) & is_mine[:, None]
    running = jnp.cumsum(onehot.astype(jnp.int32), axis=0) - 1
    rank_own = jnp.sum(jnp.where(onehot, running, 0), axis=1)
    slot = jnp.where(is_mine, target * capacity + rank_own, slot_total)
    slot_token = jnp.zeros((slot_total,), jnp.int32).at[slot].set(entry_token, mode="drop")
    filled = jnp.zeros((slot_total,), jnp.bool_).at[slot].set(True, mode="drop")
    outgoing = jnp.where(
        filled[:, None], jnp.take(normed, slot_token, axis=0), jnp.zeros((), jnp.bfloat16)
    )
    outgoing = outgoing.reshape(sp_count, capacity, model_width)
    gate_local = expert_gate[0]
    up_local = expert_up[0]
    down_local = expert_down[0]
    arrived = lax.all_to_all(outgoing, "sp", split_axis=0, concat_axis=0, tiled=True)
    source_count, slot_count, width_in = arrived.shape
    flat_rows = arrived.reshape(source_count * slot_count, width_in)
    gate_out = jnp.dot(flat_rows, gate_local, preferred_element_type=jnp.float32)
    up_out = jnp.dot(flat_rows, up_local, preferred_element_type=jnp.float32)
    expert_inner = (jax.nn.silu(gate_out) * up_out).astype(jnp.bfloat16)
    produced = jnp.dot(expert_inner, down_local, preferred_element_type=jnp.float32).astype(
        jnp.bfloat16
    )
    produced = produced.reshape(source_count, slot_count, width_in)
    returned = lax.all_to_all(produced, "sp", split_axis=0, concat_axis=0, tiled=True).reshape(
        slot_total, model_width
    )
    entry_slot = jnp.minimum(slot, slot_total - 1)
    selected = jnp.take(returned, entry_slot, axis=0).astype(jnp.float32)
    entry_scale = jnp.where(is_mine, route_weights.reshape(-1), 0.0)
    routed = (
        (selected * entry_scale[:, None]).reshape(tok_count, topk_count, model_width).sum(axis=1)
    )
    gate_part = jnp.dot(normed, shared_gate, preferred_element_type=jnp.float32)
    up_part = jnp.dot(normed, shared_up, preferred_element_type=jnp.float32)
    shared_inner = (jax.nn.silu(gate_part) * up_part).astype(jnp.bfloat16)
    mixed_rows = sent_and_summed(
        (jnp.dot(shared_inner, shared_down, preferred_element_type=jnp.float32) + routed).astype(
            jnp.bfloat16
        ),
        "tp",
        0,
    )
    return (hidden_own.astype(jnp.float32) + mixed_rows).astype(jnp.bfloat16)


def solution(mesh):
    placed = (
        P("sp", "tp"),
        P("sp", "tp"),
        P("sp", "tp"),
        P(),
        P(),
        P("tp"),
        P(),
        P("sp", None),
        P(),
        P("sp", None),
        P("sp", None),
        P(("sp", "tp"), None, None),
        P(("sp", "tp"), None, None),
        P(("sp", "tp"), None, None),
        P(None, "tp"),
        P(None, "tp"),
        P("tp", None),
    )
    return jax.shard_map(
        local, mesh=mesh, in_specs=placed, out_specs=P(("sp", "tp"), None), check_vma=False
    )
```

profile of v0, /device:TPU:32, one launch (start us, length us, event | category | flops | bytes accessed | tf_op | source)
XLA Modules:
  0.0 602.0 jit_solution(10993135226981612924)
XLA Ops:
  15.0 34.5 %reduce-window.6 = s32[64,10,128]{2,1,0:T(8,128)} reduce-window(s32[64,10,128]{2,1,0:T(8,128)} %fusion.31, s32[]{:T(128)} %constant.142.clone.1), window={size=1x1x128 pad=0_0x0_0x127_0}, to_apply=%region_8.9 | reduce-window | flops 10403840 | bytes 655364 | tf_op jit(solution)/shard_map/reduce-window
  55.0 36.8 %all-gather.2.cloned.1.call-done = bf16[20480,128]{1,0:T(8,128)(2,1)} async-done(((bf16[320,128]{1,0:T(8,128)(2,1)}), bf16[20480,128]{1,0:T(8,128)(2,1)}) %all-gather.2.cloned.1.call-update) | async-done | bytes 5242896 | tf_op jit(solution)/shard_map/all_gather | solution.py:133
  91.7 154.4 %while.15 = (s32[]{:T(128)}, f32[1280]{0:T(1024)S(1)}, f32[1280]{0:T(1024)S(1)}, f32[1280,64]{0,1:T(8,128)S(1)}, bf16[10,2048,128]{2,1,0:T(8,128)(2,1)}, /*index=5*/bf16[1280,64]{1,0:T(8,128)(2,1)S(1)}, s32[]{:T(128)}, s32[]{:T(128)}) while((s32[]{:T(128)}, f32[1280]{0:T(1024)S(1)}, f32[1280]{0:T(1024)S(1)}, ...), condition=%wide.region_5.6_spmd.clone, body=%wide.region_2.5_spmd.clone.sunk | while | flops 692312320 | bytes 76398720 | solution.py:160
  98.3 5.9 fusion.103
  113.8 5.9 fusion.103
  129.2 5.9 fusion.103
  144.7 5.9 fusion.103
  160.1 5.9 fusion.103
  175.6 5.9 fusion.103
  191.0 5.9 fusion.103
  206.4 5.9 fusion.103
  221.9 5.9 fusion.103
  237.3 5.9 fusion.103
  252.0 6.1 %all-to-all-done = bf16[4,80,256]{2,1,0:T(8,128)(2,1)S(1)} async-done(((bf16[4,80,256]{2,1,0:T(8,128)(2,1)}), bf16[4,80,256]{2,1,0:T(8,128)(2,1)S(1)}, u32[]{:S(2)}, u32[]{:S(2)}) %all-to-all-start) | async-done | bytes 163872 | tf_op jit(solution)/shard_map/all_to_all | solution.py:168
  275.1 11.2 %scatter_custom_fusion = pred[640]{0:T(1024)(128)(4,1)S(1)} fusion(s32[1280]{0:T(1024)S(1)} %get-tuple-element.80, pred[1280]{0:T(1024)(128)(4,1)S(1)} %broadcast.668, pred[]{:T(512)} %constant.167.clone.1), kind=kCustom, calls=%fused_computation.161 | custom fusion | bytes 641 | tf_op jit(solution)/shard_map/scatter | solution.py:189
  298.6 102.4 %all_to_all.39 = bf16[64,10,2048]{2,1,0:T(8,128)(2,1)} all-to-all(bf16[64,10,2048]{2,1,0:T(8,128)(2,1)S(1)} %select_select_fusion), channel_id=1, replica_groups=mesh['sp'=64,'tp'=4] {'sp'}, dimensions={0} | all-to-all | bytes 5242880 | tf_op jit(solution)/shard_map/all_to_all | solution.py:197
  411.5 7.2 %convolution_convert_fusion = bf16[640,2048]{1,0:T(8,128)(2,1)} fusion(bf16[1,512,2048]{2,1,0:T(8,128)(2,1)S(1)} %copy-done, bf16[640,2048]{1,0:T(8,128)(2,1)} %reshape.656, bf16[1,2048,512]{2,1,0:T(8,128)(2,1)} %param.31, f32[640,512]{1,0:T(8,128)} %fusion.18), kind=kOutput, calls=%fused_computation.22 | convolution fusion | flops 2687631360 | bytes 10747904 | tf_op jit(solution)/shard_map/dot_general | solution.py:203
  424.1 6.8 %all-to-all-start.3 = ((bf16[64,10,2048]{2,1,0:T(8,128)(2,1)}), bf16[64,10,2048]{2,1,0:T(8,128)(2,1)}, u32[]{:S(2)}, u32[]{:S(2)}) async-start(bf16[64,10,2048]{2,1,0:T(8,128)(2,1)} %reshape.657), calls=%async_computation.3 | async-start | bytes 8388608 | tf_op jit(solution)/shard_map/all_to_all | solution.py:207
  438.0 88.2 %all-to-all-done.3 = bf16[64,10,2048]{2,1,0:T(8,128)(2,1)} async-done(((bf16[64,10,2048]{2,1,0:T(8,128)(2,1)}), bf16[64,10,2048]{2,1,0:T(8,128)(2,1)}, u32[]{:S(2)}, u32[]{:S(2)}) %all-to-all-start.3) | async-done | bytes 2621472 | tf_op jit(solution)/shard_map/all_to_all | solution.py:207
  526.2 5.5 reshape.658
  531.8 12.9 %gather_fusion.1 = bf16[1280,2048]{1,0:T(8,128)(2,1)} fusion(bf16[640,2048]{1,0:T(8,128)(2,1)} %reshape.658, s32[2048]{0:T(1024)S(1)} %pad_clamp_fusion), kind=kCustom, calls=%fused_computation.1 | custom fusion | bytes 10490880 | tf_op jit(solution)/shard_map/jit(_take)/gather | solution.py:211
  544.7 8.7 %gather.15 = bf16[320,4,2048]{2,1,0:T(4,128)(2,1)} reshape(bf16[1280,2048]{1,0:T(8,128)(2,1)} %gather_fusion.1) | data formatting | bytes 10485760 | tf_op jit(solution)/shard_map/jit(_take)/gather | solution.py:211
  553.3 13.7 %multiply_reduce_fusion.1 = f32[320,2048]{1,0:T(8,128)} fusion(f32[320,4]{1,0:T(8,128)} %broadcast_select_fusion, bf16[320,4,2048]{2,1,0:T(4,128)(2,1)} %gather.15, pred[320,4]{1,0:T(8,128)(4,1)S(1)} %compare_and_fusion), kind=kLoop, calls=%fused_computation.20 | loop fusion | flops 9830400 | bytes 7870720 | tf_op jit(solution)/shard_map/reduce_sum | solution.py:214
  571.8 22.3 %all_to_all.40 = bf16[4,80,2048]{2,1,0:T(8,128)(2,1)S(1)} all-to-all(bf16[4,80,2048]{2,1,0:T(8,128)(2,1)} %bitcast.85), channel_id=1, replica_groups=mesh['sp'=64,'tp'=4] {'tp'}, dimensions={0} | all-to-all | bytes 2621440 | tf_op jit(solution)/shard_map/all_to_all | solution.py:39
  (177 shorter events, 172.6 us)
Async XLA Ops:
  6.5 405.0 %copy-start = (bf16[1,512,2048]{2,1,0:T(8,128)(2,1)S(1)}, bf16[1,512,2048]{2,1,0:T(8,128)(2,1)}, u32[]{:S(2)}) copy-start(bf16[1,512,2048]{2,1,0:T(8,128)(2,1)} %param.32) | copy-start | bytes 6291460
  6.5 7.5 %copy-start.8 = (f32[256]{0:T(256)S(1)}, f32[256]{0:T(256)}, u32[]{:S(2)}) copy-start(f32[256]{0:T(256)} %param.24) | copy-start | bytes 3076
  6.5 85.2 %all-gather.2.cloned.1.call-start = ((), (), s32[]{:S(2)}) async-start(), calls=%async_computation.5 | async-start | bytes 5324800 | tf_op jit(solution)/shard_map/all_gather | solution.py:133
  11.2 40.3 %copy-start.2 = (s32[320,4]{1,0:T(8,128)}, s32[320,4]{1,0:T(8,128)S(1)}, u32[]{:S(2)}) copy-start(s32[320,4]{1,0:T(8,128)S(1)} %copy.94) | copy-start | bytes 15364
  98.3 7.0 %copy-start.1 = (f32[2048,1280]{1,0:T(8,128)S(1)}, f32[2048,1280]{1,0:T(8,128)}, u32[]{:S(2)}) copy-start(f32[2048,1280]{1,0:T(8,128)} %get-tuple-element.155) | copy-start | bytes 31457284 | tf_op jit(solution)/shard_map/while
  113.8 7.0 %copy-start.1 = (f32[2048,1280]{1,0:T(8,128)S(1)}, f32[2048,1280]{1,0:T(8,128)}, u32[]{:S(2)}) copy-start(f32[2048,1280]{1,0:T(8,128)} %get-tuple-element.155) | copy-start | bytes 31457284 | tf_op jit(solution)/shard_map/while
  129.2 7.0 %copy-start.1 = (f32[2048,1280]{1,0:T(8,128)S(1)}, f32[2048,1280]{1,0:T(8,128)}, u32[]{:S(2)}) copy-start(f32[2048,1280]{1,0:T(8,128)} %get-tuple-element.155) | copy-start | bytes 31457284 | tf_op jit(solution)/shard_map/while
  144.7 7.0 %copy-start.1 = (f32[2048,1280]{1,0:T(8,128)S(1)}, f32[2048,1280]{1,0:T(8,128)}, u32[]{:S(2)}) copy-start(f32[2048,1280]{1,0:T(8,128)} %get-tuple-element.155) | copy-start | bytes 31457284 | tf_op jit(solution)/shard_map/while
  160.1 7.0 %copy-start.1 = (f32[2048,1280]{1,0:T(8,128)S(1)}, f32[2048,1280]{1,0:T(8,128)}, u32[]{:S(2)}) copy-start(f32[2048,1280]{1,0:T(8,128)} %get-tuple-element.155) | copy-start | bytes 31457284 | tf_op jit(solution)/shard_map/while
  175.6 7.0 %copy-start.1 = (f32[2048,1280]{1,0:T(8,128)S(1)}, f32[2048,1280]{1,0:T(8,128)}, u32[]{:S(2)}) copy-start(f32[2048,1280]{1,0:T(8,128)} %get-tuple-element.155) | copy-start | bytes 31457284 | tf_op jit(solution)/shard_map/while
  191.0 7.0 %copy-start.1 = (f32[2048,1280]{1,0:T(8,128)S(1)}, f32[2048,1280]{1,0:T(8,128)}, u32[]{:S(2)}) copy-start(f32[2048,1280]{1,0:T(8,128)} %get-tuple-element.155) | copy-start | bytes 31457284 | tf_op jit(solution)/shard_map/while
  206.4 7.0 %copy-start.1 = (f32[2048,1280]{1,0:T(8,128)S(1)}, f32[2048,1280]{1,0:T(8,128)}, u32[]{:S(2)}) copy-start(f32[2048,1280]{1,0:T(8,128)} %get-tuple-element.155) | copy-start | bytes 31457284 | tf_op jit(solution)/shard_map/while
  221.9 7.0 %copy-start.1 = (f32[2048,1280]{1,0:T(8,128)S(1)}, f32[2048,1280]{1,0:T(8,128)}, u32[]{:S(2)}) copy-start(f32[2048,1280]{1,0:T(8,128)} %get-tuple-element.155) | copy-start | bytes 31457284 | tf_op jit(solution)/shard_map/while
  237.3 7.0 %copy-start.1 = (f32[2048,1280]{1,0:T(8,128)S(1)}, f32[2048,1280]{1,0:T(8,128)}, u32[]{:S(2)}) copy-start(f32[2048,1280]{1,0:T(8,128)} %get-tuple-element.155) | copy-start | bytes 31457284 | tf_op jit(solution)/shard_map/while
  247.7 10.4 %all-to-all-start = ((bf16[4,80,256]{2,1,0:T(8,128)(2,1)}), bf16[4,80,256]{2,1,0:T(8,128)(2,1)S(1)}, u32[]{:S(2)}, u32[]{:S(2)}) async-start(bf16[4,80,256]{2,1,0:T(8,128)(2,1)} %copy.91), calls=%async_computation | async-start | bytes 327680 | tf_op jit(solution)/shard_map/all_to_all | solution.py:168
  258.2 4.1 copy-start.6
  261.4 0.9 copy-start.3
  263.6 22.9 %all-to-all-start.1 = ((bf16[4,80,2048]{2,1,0:T(8,128)(2,1)}), bf16[4,80,2048]{2,1,0:T(8,128)(2,1)S(1)}, u32[]{:S(2)}, u32[]{:S(2)}) async-start(bf16[4,80,2048]{2,1,0:T(8,128)(2,1)} %broadcast_in_dim.104), calls=%async_computation.1 | async-start | bytes 2621440 | tf_op jit(solution)/shard_map/all_to_all | solution.py:22
  424.1 7.7 %copy-start.5 = (s32[320,4]{0,1:T(4,128)S(1)}, s32[320,4]{0,1:T(4,128)}, u32[]{:S(2)}) copy-start(s32[320,4]{0,1:T(4,128)} %param.28) | copy-start | bytes 15364
  424.1 7.9 %copy-start.7 = (f32[320,4]{0,1:T(4,128)S(1)}, f32[320,4]{0,1:T(4,128)}, u32[]{:S(2)}) copy-start(f32[320,4]{0,1:T(4,128)} %param.29) | copy-start | bytes 15364
  424.1 102.1 %all-to-all-start.3 = ((bf16[64,10,2048]{2,1,0:T(8,128)(2,1)}), bf16[64,10,2048]{2,1,0:T(8,128)(2,1)}, u32[]{:S(2)}, u32[]{:S(2)}) async-start(bf16[64,10,2048]{2,1,0:T(8,128)(2,1)} %reshape.657), calls=%async_computation.3 | async-start | bytes 8388608 | tf_op jit(solution)/shard_map/all_to_all | solution.py:207
  571.8 22.6 %copy-start.4 = (f32[80,2048]{1,0:T(8,128)S(1)}, f32[80,2048]{1,0:T(8,128)}, u32[]{:S(2)}) copy-start(f32[80,2048]{1,0:T(8,128)} %copy-done.3) | copy-start | bytes 1966084
Sparse Core Ops, SparseCore 0:
  10.5 81.2 all-gather.1
where the time goes:
time: 607 us; the launch traced here: 602 us
  waiting for transfers between devices  131 us (22%)
  blocking collectives  125 us (21%)
  other arithmetic  122 us (20%)
  local copies, waits for them, and re-layouts  99.5 us (16%)
  matrix products  96 us (16%)
  starting transfers between devices  14.7 us (2%)
  between operations  13.8 us (2%)
    all_to_all x1, blocking collectives, local(): lax.all_to_all(outgoing, 'sp', split_axis=0, concat_axis=0, tiled=True)  102 us
    all_to_all x1, waiting for transfers between devices, local(): lax.all_to_all(produced, 'sp', split_axis=0, concat_axis=0, tiled=True)  88.2 us
    reduce_sum x10, other arithmetic, step(): new_total = run_total * factor + jnp.sum(expo_terms, axis=1)  58.8 us
    dot_general x10, matrix products, step(): lax.dot_general(query_rows, key_slab[:, :HEAD_SIZE], (((1,), (1,)), ((),...  55.1 us
    all_gather x1, waiting for transfers between devices, local(): piece = lax.all_gather(packed, 'sp', axis=0, tiled=True)  36.8 us
    another operation x4, other arithmetic  34.8 us
    all_to_all x1, blocking collectives, sent_and_summed(): tiles = lax.all_to_all(split_up(value, dim, length), axis, 0, 0, tiled=True)  22.3 us
    gather x2, local copies, waits for them, and re-layouts, local(): selected = jnp.take(returned, entry_slot, axis=0).astype(jnp.float32)  21.6 us
  transfers between devices with their start and end apart: 4, of which 3 were waited for; matrix products, arithmetic and copies ran while one was open for 12% of the time, Pallas kernels for 0%

commit v1 on v0

v1 whole, which is shorter than its diff:
```python
import functools

import jax
import jax.numpy as jnp
from jax import lax
from jax.experimental import pallas as pl
from jax.experimental.pallas import tpu as pltpu
from jax.sharding import PartitionSpec as P

HEAD_SIZE = 64
GRID_W = 64
EPS = 1e-06
THETA = 10000.0
LOG2E = 1.4426950408889634
CAPACITY = 10
SAFE_BOUND = 70.0

VM = pl.BlockSpec(memory_space=pltpu.VMEM)
SM = pl.BlockSpec(memory_space=pltpu.SMEM)


def split_up(value, dim, length):
    dims = value.shape
    tiles = value.reshape(*dims[:dim], length, dims[dim] // length, *dims[dim + 1 :])
    return jnp.moveaxis(tiles, dim, 0)


def sent_and_summed(value, axis, dim):
    length = lax.axis_size(axis)
    tiles = lax.all_to_all(split_up(value, dim, length), axis, 0, 0, tiled=True)
    return jnp.sum(tiles.astype(jnp.float32), axis=0)


def gather_rows(value, axis):
    length = lax.axis_size(axis)
    tiles = lax.all_to_all(
        jnp.broadcast_to(value[None], (length, *value.shape)), axis, 0, 0, tiled=True
    )
    return tiles.reshape(length * value.shape[0], value.shape[1])


def final_norm(field, gain):
    mean_sq = jnp.mean(field * field, axis=-1, keepdims=True)
    return field * lax.rsqrt(mean_sq + EPS) * gain


def wide_tables(positions, sequence_total):
    grid_rows = sequence_total // GRID_W
    row_pos = (positions // GRID_W - grid_rows // 2).astype(jnp.float32)
    col_pos = (positions % GRID_W - GRID_W // 2).astype(jnp.float32)
    quarter = HEAD_SIZE // 4
    inverse = THETA ** (-jnp.arange(quarter, dtype=jnp.float32) / quarter)
    lane = jnp.arange(2 * HEAD_SIZE, dtype=jnp.int32)
    inverse_wide = jnp.tile(inverse, 8)
    is_row = (lane % HEAD_SIZE) < HEAD_SIZE // 2
    angles = jnp.where(is_row[None, :], row_pos[:, None], col_pos[:, None]) * inverse_wide
    sign = jnp.where((lane % 32) < 16, -1.0, 1.0)
    return jnp.cos(angles), jnp.sin(angles) * sign[None, :]


def normed_and_turned(field, gain, cosine, sine):
    lane = lax.broadcasted_iota(jnp.int32, field.shape, 1)
    low = lane < HEAD_SIZE
    square = field * field
    mean_low = jnp.sum(jnp.where(low, square, 0.0), axis=1, keepdims=True) / HEAD_SIZE
    mean_high = jnp.sum(jnp.where(low, 0.0, square), axis=1, keepdims=True) / HEAD_SIZE
    scale = jnp.where(low, lax.rsqrt(mean_low + EPS), lax.rsqrt(mean_high + EPS))
    unit = field * scale * gain
    partner = jnp.where(
        lane % 32 < 16, pltpu.roll(unit, 128 - 16, 1), pltpu.roll(unit, 16, 1)
    )
    return unit * cosine + partner * sine


def prepare_kernel(q_ref, kv_ref, qg_ref, kg_ref, cos_ref, sin_ref, rows_ref, packed_ref):
    tokens = q_ref.shape[0]
    cosine, sine = cos_ref[...], sin_ref[...]
    low = lax.broadcasted_iota(jnp.int32, (tokens, 128), 1) < HEAD_SIZE
    both = kv_ref[...].astype(jnp.float32)
    turned = normed_and_turned(both, kg_ref[...], cosine, sine)
    packed_ref[...] = jnp.where(low, turned, both).astype(jnp.bfloat16)
    for pair in range(q_ref.shape[1] // 128):
        field = q_ref[:, pair * 128 : (pair + 1) * 128].astype(jnp.float32)
        turned = normed_and_turned(field, qg_ref[...], cosine, sine).astype(jnp.bfloat16)
        turned = turned.astype(jnp.float32) * (HEAD_SIZE**-0.5)
        first = jnp.where(low, turned, 0.0)
        second = jnp.where(low, pltpu.roll(turned, HEAD_SIZE, 1), 0.0)
        rows_ref[(2 * pair) * tokens : (2 * pair + 1) * tokens, :] = first.astype(jnp.bfloat16)
        rows_ref[(2 * pair + 1) * tokens : (2 * pair + 2) * tokens, :] = second.astype(jnp.bfloat16)


def attention_kernel(block, flag_ref, q_ref, kv_ref, gain_ref, out_ref, acc_ref, sum_ref, max_ref):
    columns = q_ref.shape[0]
    steps = kv_ref.shape[0] // block
    acc_ref[...] = jnp.zeros_like(acc_ref)
    sum_ref[...] = jnp.zeros_like(sum_ref)

    def scores_of(step):
        slab = kv_ref[pl.ds(pl.multiple_of(step * block, block), block), :]
        scores = lax.dot_general(
            slab, q_ref[...], (((1,), (1,)), ((), ())), preferred_element_type=jnp.float32
        )
        return slab, scores

    def weighed(slab, weights):
        return lax.dot_general(
            slab,
            weights.astype(jnp.bfloat16),
            (((0,), (0,)), ((), ())),
            preferred_element_type=jnp.float32,
        )[HEAD_SIZE:]

    def plain_step(step, carry):
        slab, scores = scores_of(step)
        weights = jnp.exp2(scores * LOG2E)
        sum_ref[...] += jnp.sum(weights.reshape(block // 8, 8, columns), axis=0)
        acc_ref[...] += weighed(slab, weights)
        return carry

    def guarded_step(step, carry):
        slab, scores = scores_of(step)
        before = max_ref[...]
        top = jnp.maximum(before, jnp.max(scores, axis=0, keepdims=True))
        factor = jnp.exp(before - top)
        weights = jnp.exp(scores - top)
        sum_ref[...] = sum_ref[...] * factor + jnp.sum(
            weights.reshape(block // 8, 8, columns), axis=0
        )
        acc_ref[...] = acc_ref[...] * factor + weighed(slab, weights)
        max_ref[...] = top
        return carry

    @pl.when(flag_ref[0] == 0)
    def _():
        lax.fori_loop(0, steps, plain_step, 0)

    @pl.when(flag_ref[0] != 0)
    def _():
        max_ref[...] = jnp.full_like(max_ref, -1e30)
        lax.fori_loop(0, steps, guarded_step, 0)

    attended = acc_ref[...] / jnp.sum(sum_ref[...], axis=0, keepdims=True)
    mean_sq = jnp.mean(attended * attended, axis=0, keepdims=True)
    unit = attended * lax.rsqrt(mean_sq + EPS)
    turned = jnp.concatenate([unit, jnp.zeros_like(unit)], axis=0).T
    tokens = out_ref.shape[0]
    low = lax.broadcasted_iota(jnp.int32, (tokens, 128), 1) < HEAD_SIZE
    for pair in range(out_ref.shape[1] // 128):
        first = turned[(2 * pair) * tokens : (2 * pair + 1) * tokens, :]
        second = turned[(2 * pair + 1) * tokens : (2 * pair + 2) * tokens, :]
        joined = jnp.where(low, first, pltpu.roll(second, HEAD_SIZE, 1))
        lanes = slice(pair * 128, (pair + 1) * 128)
        out_ref[:, lanes] = (joined * gain_ref[:, lanes]).astype(jnp.bfloat16)


def dispatch_kernel(code_ref, normed_ref, out_ref):
    tokens, width = normed_ref.shape
    rows = out_ref.shape[0]
    quarter = width // 4
    row = lax.broadcasted_iota(jnp.int32, (rows, tokens), 0)
    main_code = (row // 8) * 16 + row % 8
    extra_code = (row // 8) * 16 + 8 + (row % 8) // 4
    main = jnp.zeros((rows, tokens), jnp.float32)
    extra = jnp.zeros((rows, tokens), jnp.float32)
    for k in range(code_ref.shape[0]):
        own = code_ref[k : k + 1, :]
        main += jnp.where(main_code == own, 1.0, 0.0)
        extra += jnp.where(extra_code == own, 1.0, 0.0)
    main = main.astype(jnp.bfloat16)
    for q in range(4):
        cols = slice(q * quarter, (q + 1) * quarter)
        out_ref[:, cols] = jnp.dot(
            main, normed_ref[:, cols], preferred_element_type=jnp.float32
        ).astype(jnp.bfloat16)
    total = jnp.zeros((rows, quarter), jnp.float32)
    for q in range(4):
        part = jnp.where(row % 4 == q, extra, 0.0).astype(jnp.bfloat16)
        total += jnp.dot(
            part,
            normed_ref[:, q * quarter : (q + 1) * quarter],
            preferred_element_type=jnp.float32,
        )
    out_ref[:, width:] = total.astype(jnp.bfloat16)


def expert_kernel(in_ref, gate_ref, up_ref, down_ref, out_ref, rows_ref, inner_ref):
    rows = in_ref.shape[0]
    width = gate_ref.shape[0]
    quarter = width // 4
    extra_rows = rows // 4
    rows_ref[:rows, :] = in_ref[:, :width]
    tail = in_ref[:, width:]
    place = lax.broadcasted_iota(jnp.int32, (extra_rows, rows), 1)
    index = lax.broadcasted_iota(jnp.int32, (extra_rows, rows), 0)
    for q in range(4):
        pick = jnp.where(place == 4 * index + q, 1.0, 0.0).astype(jnp.bfloat16)
        rows_ref[rows:, q * quarter : (q + 1) * quarter] = jnp.dot(
            pick, tail, preferred_element_type=jnp.float32
        ).astype(jnp.bfloat16)
    every = rows_ref[...]
    gate = jnp.dot(every, gate_ref[...], preferred_element_type=jnp.float32)
    up = jnp.dot(every, up_ref[...], preferred_element_type=jnp.float32)
    inner_ref[...] = (gate / (1.0 + jnp.exp(-gate)) * up).astype(jnp.bfloat16)
    place = lax.broadcasted_iota(jnp.int32, (rows, extra_rows), 0)
    index = lax.broadcasted_iota(jnp.int32, (rows, extra_rows), 1)
    total = jnp.zeros((rows, quarter), jnp.float32)
    for q in range(4):
        cols = slice(q * quarter, (q + 1) * quarter)
        made = jnp.dot(
            inner_ref[...], down_ref[:, cols], preferred_element_type=jnp.float32
        ).astype(jnp.bfloat16)
        out_ref[:, cols] = made[:rows]
        pick = jnp.where(place == 4 * index + q, 1.0, 0.0).astype(jnp.bfloat16)
        total += jnp.dot(pick, made[rows:], preferred_element_type=jnp.float32)
    out_ref[:, width:] = total.astype(jnp.bfloat16)


def combine_kernel(code_ref, weight_ref, back_ref, inner_ref, down_ref, out_ref):
    tokens, width = out_ref.shape
    rows = back_ref.shape[0]
    quarter = width // 4
    place = lax.broadcasted_iota(jnp.int32, (tokens, rows), 1)
    main_code = (place // 8) * 16 + place % 8
    extra_code = (place // 8) * 16 + 8 + (place % 8) // 4
    main = jnp.zeros((tokens, rows), jnp.float32)
    extra = jnp.zeros((tokens, rows), jnp.float32)
    for k in range(code_ref.shape[1]):
        own = code_ref[:, k : k + 1]
        scale = weight_ref[:, k : k + 1]
        main += jnp.where(main_code == own, scale, 0.0)
        extra += jnp.where(extra_code == own, scale, 0.0)

    def parts_of(value):
        high = value.astype(jnp.bfloat16)
        return high, (value - high.astype(jnp.float32)).astype(jnp.bfloat16)

    high, low = parts_of(main)
    tail = back_ref[:, width:]
    for q in range(4):
        cols = slice(q * quarter, (q + 1) * quarter)
        own_high, own_low = parts_of(jnp.where(place % 4 == q, extra, 0.0))
        total = jnp.dot(inner_ref[...], down_ref[:, cols], preferred_element_type=jnp.float32)
        total += jnp.dot(high, back_ref[:, cols], preferred_element_type=jnp.float32)
        total += jnp.dot(low, back_ref[:, cols], preferred_element_type=jnp.float32)
        total += jnp.dot(own_high, tail, preferred_element_type=jnp.float32)
        total += jnp.dot(own_low, tail, preferred_element_type=jnp.float32)
        out_ref[:, cols] = total.astype(jnp.bfloat16)


def call(kernel, out_shape, args, specs=None, scratch=(), flops=0, moved=0):
    return pl.pallas_call(
        kernel,
        out_shape=out_shape,
        in_specs=specs or [VM] * len(args),
        out_specs=jax.tree.map(lambda _: VM, out_shape),
        scratch_shapes=scratch,
        compiler_params=pltpu.CompilerParams(vmem_limit_bytes=56 * 2**20),
        cost_estimate=pl.CostEstimate(flops=flops, bytes_accessed=moved, transcendentals=0),
    )(*args)


def shaped(dims, kind=jnp.bfloat16):
    return jax.ShapeDtypeStruct(dims, kind)


def slot_codes(routes, tp_index, tp_count, sp_count):
    tokens, top = routes.shape
    flat = routes.reshape(-1)
    is_mine = flat % tp_count == tp_index
    target = flat // tp_count
    onehot = (target[:, None] == jnp.arange(sp_count, dtype=jnp.int32)[None, :]) & is_mine[:, None]
    hot = onehot.astype(jnp.bfloat16)
    entries = tokens * top
    order = jnp.arange(entries, dtype=jnp.int32)
    before = (order[:, None] > order[None, :]).astype(jnp.bfloat16)
    earlier = jnp.dot(before, hot, preferred_element_type=jnp.float32)
    rank = jnp.sum(jnp.where(onehot, earlier, 0.0), axis=1).astype(jnp.int32)
    return jnp.where(is_mine, target * 16 + rank, -1).reshape(tokens, top)


def local(
    queries,
    key_matrix,
    values,
    query_gain,
    key_norm_gain,
    head_gain,
    out_proj,
    residual,
    ffn_gain,
    routes,
    route_weights,
    expert_gate,
    expert_up,
    expert_down,
    shared_gate,
    shared_up,
    shared_down,
):
    tokens = queries.shape[0]
    heads = queries.shape[1] // HEAD_SIZE
    sp_count = lax.axis_size("sp")
    tp_count = lax.axis_size("tp")
    tp_index = lax.axis_index("tp")
    sequence_total = tokens * sp_count
    positions = lax.axis_index("sp") * tokens + jnp.arange(tokens, dtype=jnp.int32)
    cosine, sine = wide_tables(positions, sequence_total)
    columns = heads * tokens
    query_rows, packed = call(
        prepare_kernel,
        (shaped((columns, 128)), shaped((tokens, 128))),
        (
            queries,
            jnp.concatenate([key_matrix, values], axis=1),
            jnp.tile(query_gain, 2)[None],
            jnp.tile(key_norm_gain, 2)[None],
            cosine,
            sine,
        ),
    )
    gathered = lax.all_gather(packed, "sp", axis=0, tiled=True)
    codes = slot_codes(routes, tp_index, tp_count, sp_count)
    bound = 8.0 * jnp.max(jnp.abs(query_gain)) * jnp.max(jnp.abs(key_norm_gain))
    wide = (bound > SAFE_BOUND).astype(jnp.int32)[None]
    head_out = call(
        functools.partial(attention_kernel, 1024),
        shaped((tokens, heads * HEAD_SIZE)),
        (wide, query_rows, gathered, head_gain[None]),
        specs=[SM, VM, VM, VM],
        scratch=(
            pltpu.VMEM((HEAD_SIZE, columns), jnp.float32),
            pltpu.VMEM((8, columns), jnp.float32),
            pltpu.VMEM((1, columns), jnp.float32),
        ),
        flops=4 * columns * sequence_total * 128,
        moved=sequence_total * 256,
    )
    part_rows = tokens // tp_count
    token_heads = lax.all_to_all(head_out, "tp", split_axis=0, concat_axis=1, tiled=True)
    own_resid = lax.dynamic_slice_in_dim(residual, tp_index * part_rows, part_rows, 0)
    hidden_own = (
        own_resid.astype(jnp.float32)
        + jnp.dot(token_heads, out_proj, preferred_element_type=jnp.float32)
    ).astype(jnp.bfloat16)
    normed_own = final_norm(hidden_own.astype(jnp.float32), ffn_gain).astype(jnp.bfloat16)
    normed = gather_rows(normed_own, "tp")
    width = normed.shape[1]
    rows = sp_count * 8
    wide_row = width + width // 4
    outgoing = call(
        dispatch_kernel,
        shaped((rows, wide_row)),
        (codes.T, normed),
        flops=4 * rows * tokens * width,
        moved=rows * wide_row * 2,
    )
    arrived = lax.all_to_all(
        outgoing.reshape(sp_count, 8, wide_row), "sp", split_axis=0, concat_axis=0, tiled=True
    )
    hidden_units = expert_gate.shape[2]
    produced = call(
        expert_kernel,
        shaped((rows, wide_row)),
        (arrived.reshape(rows, wide_row), expert_gate[0], expert_up[0], expert_down[0]),
        scratch=(
            pltpu.VMEM((rows + rows // 4, width), jnp.bfloat16),
            pltpu.VMEM((rows + rows // 4, hidden_units), jnp.bfloat16),
        ),
        flops=6 * rows * width * hidden_units,
        moved=3 * width * hidden_units * 2,
    )
    returned = lax.all_to_all(
        produced.reshape(sp_count, 8, wide_row), "sp", split_axis=0, concat_axis=0, tiled=True
    ).reshape(rows, wide_row)
    gate_part = jnp.dot(normed, shared_gate, preferred_element_type=jnp.float32)
    up_part = jnp.dot(normed, shared_up, preferred_element_type=jnp.float32)
    shared_inner = (jax.nn.silu(gate_part) * up_part).astype(jnp.bfloat16)
    partial = call(
        combine_kernel,
        shaped((tokens, width)),
        (codes, route_weights, returned, shared_inner, shared_down),
        flops=5 * tokens * rows * width,
        moved=rows * wide_row * 2,
    )
    mixed = sent_and_summed(partial, "tp", 0)
    return (hidden_own.astype(jnp.float32) + mixed).astype(jnp.bfloat16)


def solution(mesh):
    placed = (
        P("sp", "tp"),
        P("sp", "tp"),
        P("sp", "tp"),
        P(),
        P(),
        P("tp"),
        P(),
        P("sp", None),
        P(),
        P("sp", None),
        P("sp", None),
        P(("sp", "tp"), None, None),
        P(("sp", "tp"), None, None),
        P(("sp", "tp"), None, None),
        P(None, "tp"),
        P(None, "tp"),
        P("tp", None),
    )
    return jax.shard_map(
        local, mesh=mesh, in_specs=placed, out_specs=P(("sp", "tp"), None), check_vma=False
    )
```

time: 607 us -> 375 us (0.62)
  other arithmetic: 122 us -> 6.71 us
  local copies, waits for them, and re-layouts: 99.5 us -> 9.09 us
  matrix products: 96 us -> 5.71 us
  Pallas kernels: 0 us -> 75 us
  blocking collectives: 125 us -> 90.6 us
  waiting for transfers between devices: 131 us -> 157 us
    dot_general x23 -> x2, matrix products: 90.6 us -> 1.99 us  [the longest x1 1.16 us: local(): up_part = jnp.dot(normed, shared_up, preferred_element_type=jnp.float32)]
    pallas_call x0 -> x5, Pallas kernels: none -> 75 us  [call(): pl.pallas_call(kernel, out_shape=out_shape, in_specs=specs or [VM] * len(...]
    reduce_sum x15 -> x0, other arithmetic: 74.8 us -> none  [the longest x10 58.8 us: step(): new_total = run_total * factor + jnp.sum(expo_terms, axis=1)]
    all_gather x1, waiting for transfers between devices: 36.8 us -> 77.4 us  [local(): gathered = lax.all_gather(packed, 'sp', axis=0, tiled=True)]
    another operation x4 -> x0, other arithmetic: 34.8 us -> none
    all_to_all x1, blocking collectives: 102 us -> 68.9 us  [local(): lax.all_to_all(outgoing.reshape(sp_count, 8, wide_row), 'sp', split_axis=...]
    gather x4 -> x0, local copies, waits for them, and re-layouts: 31 us -> none  [the longest x2 21.6 us: local(): selected = jnp.take(returned, entry_slot, axis=0).astype(jnp.float32)]
    reshape x7 -> x1, local copies, waits for them, and re-layouts: 18 us -> 0.14 us  [slot_codes(): flat = routes.reshape(-1)]
  transfers between devices with their start and end apart: 4 -> 4, of which waited for: 3 -> 4; matrix products, arithmetic and copies ran while one was open for 12% -> 2% of each run, Pallas kernels for 0% -> 0%
where the time goes in v1:
time: 375 us; the launch traced here: 374 us
  waiting for transfers between devices  157 us (42%)
  blocking collectives  90.6 us (24%)
  Pallas kernels  75 us (20%)
  between operations  14.9 us (4%)
  starting transfers between devices  14.8 us (4%)
  local copies, waits for them, and re-layouts  9.09 us (2%)
  other arithmetic  6.71 us (2%)
  matrix products  5.71 us (2%)
    all_gather x1, waiting for transfers between devices, local(): gathered = lax.all_gather(packed, 'sp', axis=0, tiled=True)  77.4 us
    pallas_call x5, Pallas kernels, call(): pl.pallas_call(kernel, out_shape=out_shape, in_specs=specs or [VM] * len(...  75 us
    all_to_all x1, blocking collectives, local(): lax.all_to_all(outgoing.reshape(sp_count, 8, wide_row), 'sp', split_axis=...  68.9 us
    all_to_all x1, waiting for transfers between devices, local(): lax.all_to_all(produced.reshape(sp_count, 8, wide_row), 'sp', split_axis=...  59 us
    all_to_all x1, blocking collectives, sent_and_summed(): tiles = lax.all_to_all(split_up(value, dim, length), axis, 0, 0, tiled=True)  21.7 us
    all_to_all x1, waiting for transfers between devices, gather_rows(): lax.all_to_all(jnp.broadcast_to(value[None], (length, *value.shape)), axi...  15 us
  transfers between devices with their start and end apart: 4, of which 4 were waited for; matrix products, arithmetic and copies ran while one was open for 2% of the time, Pallas kernels for 0%

profile of v1, /device:TPU:32, one launch (start us, length us, event | category | flops | bytes accessed | tf_op | source)
XLA Modules:
  0.0 374.1 jit_solution(1898220699467874352)
XLA Ops:
  6.7 0.9 copy.42
  7.6 0.9 copy.43
  11.9 1.9 sine_multiply_fusion
  13.8 2.7 shard_map.163
  16.6 1.3 abs_reduce_fusion.1
  18.5 1.3 abs_reduce_fusion
  20.5 77.4 %all-gather.2.cloned.1.call-done.kv_ref = bf16[20480,128]{1,0:T(8,128)(2,1)} async-done(((bf16[320,128]{1,0:T(8,128)(2,1)}), bf16[20480,128]{1,0:T(8,128)(2,1)}) %all-gather.2.cloned.1.call-update) | async-done | bytes 5242896 | tf_op jit(solution)/shard_map/all_gather | solution.py:321
  97.9 49.3 %shard_map.164 = bf16[320,256]{1,0:T(8,128)(2,1)} custom-call(s32[1]{0:T(128)} %bitcast.flag_ref, bf16[1280,128]{1,0:T(8,128)(2,1)} %get-tuple-element.7.q_ref, bf16[20480,128]{1,0:T(8,128)(2,1)} %all-gather.2.cloned.1.call-done.kv_ref, f32[1,256]{1,0:T(1,128)} %bitcast.36), custom_call_target="tpu_custom_call" | custom-call | flops 13421772800 | bytes 5242880 | tf_op jit(solution)/shard_map/pallas_call | solution.py:251
  147.2 4.3 %all-to-all-start = ((bf16[4,80,256]{2,1,0:T(8,128)(2,1)}), bf16[4,80,256]{2,1,0:T(8,128)(2,1)S(1)}, u32[]{:S(2)}, u32[]{:S(2)}) async-start(bf16[4,80,256]{2,1,0:T(8,128)(2,1)} %bitcast.32), calls=%async_computation | async-start | bytes 327680 | tf_op jit(solution)/shard_map/all_to_all | solution.py:339
  151.8 5.9 %all-to-all-done = bf16[4,80,256]{2,1,0:T(8,128)(2,1)S(1)} async-done(((bf16[4,80,256]{2,1,0:T(8,128)(2,1)}), bf16[4,80,256]{2,1,0:T(8,128)(2,1)S(1)}, u32[]{:S(2)}, u32[]{:S(2)}) %all-to-all-start) | async-done | bytes 163872 | tf_op jit(solution)/shard_map/all_to_all | solution.py:339
  157.6 3.2 multiply_reduce_fusion
  161.0 1.2 broadcast_in_dim.72
  162.3 3.5 all-to-all-start.1
  167.9 15.0 %all-to-all-done.1 = bf16[4,80,2048]{2,1,0:T(8,128)(2,1)S(1)} async-done(((bf16[4,80,2048]{2,1,0:T(8,128)(2,1)}), bf16[4,80,2048]{2,1,0:T(8,128)(2,1)S(1)}, u32[]{:S(2)}, u32[]{:S(2)}) %all-to-all-start.1) | async-done | bytes 1310752 | tf_op jit(solution)/shard_map/all_to_all | solution.py:36
  183.0 1.1 copy-done.1
  184.1 5.6 %shard_map.165 = bf16[512,2560]{1,0:T(8,128)(2,1)} custom-call(s32[4,320]{1,0:T(4,128)} %copy.53.code_ref, bf16[320,2048]{1,0:T(8,128)(2,1)} %bitcast.22), custom_call_target="tpu_custom_call" | custom-call | flops 1342177280 | bytes 2621440 | tf_op jit(solution)/shard_map/pallas_call | solution.py:251
  189.7 68.9 %all_to_all.39 = bf16[64,8,2560]{2,1,0:T(8,128)(2,1)} all-to-all(bf16[64,8,2560]{2,1,0:T(8,128)(2,1)} %bitcast.26), channel_id=1, replica_groups=mesh['sp'=64,'tp'=4] {'sp'}, dimensions={0} | all-to-all | bytes 5242880 | tf_op jit(solution)/shard_map/all_to_all | solution.py:357
  258.6 10.6 %shard_map.166 = bf16[512,2560]{1,0:T(8,128)(2,1)} custom-call(bf16[512,2560]{1,0:T(8,128)(2,1)} %bitcast.27, bf16[2048,512]{1,0:T(8,128)(2,1)} %bitcast.33, bf16[2048,512]{1,0:T(8,128)(2,1)} %bitcast.34, bf16[512,2048]{1,0:T(8,128)(2,1)} %bitcast.35), custom_call_target="tpu_custom_call" | custom-call | flops 3221225472 | bytes 6291456 | tf_op jit(solution)/shard_map/pallas_call | solution.py:251
  269.2 7.0 %all-to-all-start.3 = ((bf16[64,8,2560]{2,1,0:T(8,128)(2,1)}), bf16[64,8,2560]{2,1,0:T(8,128)(2,1)}, u32[]{:S(2)}, u32[]{:S(2)}) async-start(bf16[64,8,2560]{2,1,0:T(8,128)(2,1)} %bitcast.25), calls=%async_computation.3 | async-start | bytes 5242880 | tf_op jit(solution)/shard_map/all_to_all | solution.py:372
  276.2 0.8 copy.54.weight_ref
  277.6 1.2 fusion.5.inner_ref
  278.7 59.0 %all-to-all-done.3 = bf16[64,8,2560]{2,1,0:T(8,128)(2,1)} async-done(((bf16[64,8,2560]{2,1,0:T(8,128)(2,1)}), bf16[64,8,2560]{2,1,0:T(8,128)(2,1)}, u32[]{:S(2)}, u32[]{:S(2)}) %all-to-all-start.3) | async-done | bytes 2621472 | tf_op jit(solution)/shard_map/all_to_all | solution.py:372
  337.7 6.8 %shard_map.167 = bf16[320,2048]{1,0:T(8,128)(2,1)} custom-call(s32[320,4]{1,0:T(8,128)} %copy-done.3, f32[320,4]{1,0:T(8,128)} %copy.54.weight_ref, bf16[512,2560]{1,0:T(8,128)(2,1)} %bitcast.12.back_ref, bf16[320,128]{1,0:T(8,128)(2,1)} %fusion.5.inner_ref, bf16[128,2048]{1,0:T(8,128)(2,1)} %down_ref.1), custom_call_target="tpu_custom_call" | custom-call | flops 1677721600 | bytes 2621440 | tf_op jit(solution)/shard_map/pallas_call | solution.py:251
  344.5 21.7 %all_to_all.40 = bf16[4,80,2048]{2,1,0:T(8,128)(2,1)S(1)} all-to-all(bf16[4,80,2048]{2,1,0:T(8,128)(2,1)} %bitcast.28), channel_id=1, replica_groups=mesh['sp'=64,'tp'=4] {'tp'}, dimensions={0} | all-to-all | bytes 2621440 | tf_op jit(solution)/shard_map/all_to_all | solution.py:30
  (45 shorter events, 7.5 us)
Async XLA Ops:
  6.5 270.5 %copy-start = (bf16[2048,128]{1,0:T(8,128)(2,1)S(1)}, bf16[2048,128]{1,0:T(8,128)(2,1)}, u32[]{:S(2)}) copy-start(bf16[2048,128]{1,0:T(8,128)(2,1)} %param.31) | copy-start | bytes 1572868
  6.5 91.4 %all-gather.2.cloned.1.call-start = ((), (), s32[]{:S(2)}) async-start(), calls=%async_computation.5 | async-start | bytes 5324800 | tf_op jit(solution)/shard_map/all_gather | solution.py:321
  97.9 53.6 %copy-start.4 = (s32[320,4]{0,1:T(4,128)S(1)}, s32[320,4]{0,1:T(4,128)}, u32[]{:S(2)}) copy-start(s32[320,4]{0,1:T(4,128)} %param.26) | copy-start | bytes 15364
  147.2 10.4 %all-to-all-start = ((bf16[4,80,256]{2,1,0:T(8,128)(2,1)}), bf16[4,80,256]{2,1,0:T(8,128)(2,1)S(1)}, u32[]{:S(2)}, u32[]{:S(2)}) async-start(bf16[4,80,256]{2,1,0:T(8,128)(2,1)} %bitcast.32), calls=%async_computation | async-start | bytes 327680 | tf_op jit(solution)/shard_map/all_to_all | solution.py:339
  157.6 3.3 copy-start.5
  162.3 20.7 %all-to-all-start.1 = ((bf16[4,80,2048]{2,1,0:T(8,128)(2,1)}), bf16[4,80,2048]{2,1,0:T(8,128)(2,1)S(1)}, u32[]{:S(2)}, u32[]{:S(2)}) async-start(bf16[4,80,2048]{2,1,0:T(8,128)(2,1)} %broadcast_in_dim.72), calls=%async_computation.1 | async-start | bytes 2621440 | tf_op jit(solution)/shard_map/all_to_all | solution.py:36
  167.2 22.4 %copy-start.3 = (s32[320,4]{1,0:T(8,128)}, s32[320,4]{1,0:T(8,128)S(1)}, u32[]{:S(2)}) copy-start(s32[320,4]{1,0:T(8,128)S(1)} %fusion.11.code_ref) | copy-start | bytes 15364
  182.9 1.1 copy-start.1
  269.2 7.0 %copy-start.6 = (f32[320,4]{0,1:T(4,128)S(1)}, f32[320,4]{0,1:T(4,128)}, u32[]{:S(2)}) copy-start(f32[320,4]{0,1:T(4,128)} %param.27) | copy-start | bytes 15364
  269.2 7.9 %copy-start.2 = (bf16[4,80,2048]{2,1,0:T(8,128)(2,1)S(1)}, bf16[4,80,2048]{2,1,0:T(8,128)(2,1)}, u32[]{:S(2)}) copy-start(bf16[4,80,2048]{2,1,0:T(8,128)(2,1)} %copy-done.1) | copy-start | bytes 3932164
  269.2 68.6 %all-to-all-start.3 = ((bf16[64,8,2560]{2,1,0:T(8,128)(2,1)}), bf16[64,8,2560]{2,1,0:T(8,128)(2,1)}, u32[]{:S(2)}, u32[]{:S(2)}) async-start(bf16[64,8,2560]{2,1,0:T(8,128)(2,1)} %bitcast.25), calls=%async_computation.3 | async-start | bytes 5242880 | tf_op jit(solution)/shard_map/all_to_all | solution.py:372
  276.2 1.4 copy-start.7
Sparse Core Ops, SparseCore 0:
  16.7 81.1 all-gather.1

commit v2 on v1

--- a/solution.py
+++ b/solution.py
@@ -89,68 +89,204 @@
         rows_ref[(2 * pair + 1) * tokens : (2 * pair + 2) * tokens, :] = second.astype(jnp.bfloat16)
 
 
-def attention_kernel(block, flag_ref, q_ref, kv_ref, gain_ref, out_ref, acc_ref, sum_ref, max_ref):
+MESH = pl.DeviceIdType.MESH
+Z_RING, X_RING = 8, 4
+
+
+def ring_attention_kernel(
+    guarded,
+    q_ref,
+    packed_ref,
+    gain_ref,
+    out_ref,
+    kv_ref,
+    mine_ref,
+    acc_ref,
+    sum_ref,
+    max_ref,
+    x_send,
+    x_recv,
+    z_send,
+    z_recv,
+    p_send,
+    p_recv,
+    t_send,
+    t_recv,
+    l_sem,
+):
+    tokens = packed_ref.shape[0]
     columns = q_ref.shape[0]
-    steps = kv_ref.shape[0] // block
+    group = X_RING * tokens
+    sp, tp = lax.axis_index("sp"), lax.axis_index("tp")
+    tp_count = lax.axis_size("tp")
+    core = sp % 2
+    x = (sp // 2) % X_RING
+    z = sp // (2 * X_RING)
+
+    def device(z_at, x_at, core_at):
+        return {"sp": ((z_at % Z_RING) * X_RING + x_at % X_RING) * 2 + core_at}
+
+    barrier = pltpu.get_barrier_semaphore()
+    others = [device(z, x + r, core) for r in range(1, X_RING)]
+    others += [device(z + 1, x, core), device(z + Z_RING - 1, x, core), device(z, x, 1 - core)]
+    others += [{"tp": (tp + r) % tp_count} for r in range(1, tp_count)]
+    for other in others:
+        pl.semaphore_signal(barrier, inc=1, device_id=other, device_id_type=MESH)
+    pl.semaphore_wait(barrier, len(others))
+
+    def slot(x_at):
+        return kv_ref.at[z, core, pl.ds(pl.multiple_of((x_at % X_RING) * tokens, tokens), tokens)]
+
+    def remote(src, dst, send_sem, recv_sem, to):
+        return pltpu.make_async_remote_copy(
+            src_ref=src,
+            dst_ref=dst,
+            send_sem=send_sem,
+            recv_sem=recv_sem,
+            device_id=to,
+            device_id_type=MESH,
+        )
+
+    def x_copy(r, source_x):
+        place = slot(source_x)
+        return remote(
+            packed_ref, place, x_send.at[r - 1], x_recv.at[r - 1], device(z, x + r, core)
+        )
+
+    def z_copy(way, hop, z_from):
+        rows = pl.ds(0, group)
+        if hop == Z_RING // 2 - 1:
+            rows = pl.ds(way * (group // 2), group // 2)
+        place = kv_ref.at[z_from % Z_RING, core, rows]
+        to = device(z + (1 if way == 0 else Z_RING - 1), x, core)
+        return remote(place, place, z_send.at[way, hop], z_recv.at[way, hop], to)
+
+    def z_out(way, hop):
+        return z_copy(way, hop, z + (Z_RING - hop if way == 0 else hop))
+
+    def z_in(way, hop):
+        return z_copy(way, hop, z + (Z_RING - 1 - hop if way == 0 else 1 + hop))
+
+    def p_copy(number, z_at, core_at):
+        place = kv_ref.at[z_at % Z_RING, core_at]
+        return remote(
+            place, place, p_send.at[number], p_recv.at[number], device(z, x, 1 - core)
+        )
+
+    def p_out(number):
+        distance = (number + 1) // 2
+        return p_copy(number, z + (Z_RING - distance if number % 2 else distance), core)
+
+    own = pltpu.make_async_copy(packed_ref, slot(x), l_sem)
+    own.start()
+    for r in range(1, X_RING):
+        x_copy(r, x).start()
     acc_ref[...] = jnp.zeros_like(acc_ref)
     sum_ref[...] = jnp.zeros_like(sum_ref)
-
-    def scores_of(step):
-        slab = kv_ref[pl.ds(pl.multiple_of(step * block, block), block), :]
+    if guarded:
+        max_ref[...] = jnp.full_like(max_ref, -1e30)
+    own.wait()
+    for r in range(1, X_RING):
+        x_copy(r, x + X_RING - r).wait_recv()
+    z_out(0, 0).start()
+    z_out(1, 0).start()
+    p_out(0).start()
+
+    def step(j, carry):
+        i = j + 2
+        distance, member = i // 4, i % 4
+        z_at = (z + Z_RING + distance * (2 * (member // 2) - 1)) % Z_RING
+        core_at = (core + member % 2) % 2
+
+        for hop in range(Z_RING // 2):
+
+            @pl.when(j == 4 * hop + 2)
+            def _(hop=hop):
+                z_in(0, hop).wait_recv()
+                z_in(1, hop).wait_recv()
+                if hop < Z_RING // 2 - 1:
+                    z_out(0, hop + 1).start()
+                    z_out(1, hop + 1).start()
+                    p_out(2 * hop + 1).start()
+                    p_out(2 * hop + 2).start()
+                else:
+                    p_out(2 * hop + 1).start()
+
+        @pl.when(member % 2 == 1)
+        def _():
+            p_copy(j // 2, z_at, 1 - core).wait_recv()
+
+        slab = kv_ref[z_at, core_at]
         scores = lax.dot_general(
             slab, q_ref[...], (((1,), (1,)), ((), ())), preferred_element_type=jnp.float32
         )
-        return slab, scores
-
-    def weighed(slab, weights):
-        return lax.dot_general(
+        if guarded:
+            before = max_ref[...]
+            top = jnp.maximum(before, jnp.max(scores, axis=0, keepdims=True))
+            factor = jnp.exp(before - top)
+            weights = jnp.exp(scores - top)
+            max_ref[...] = top
+        else:
+            factor = None
+            weights = jnp.exp2(scores * LOG2E)
+        added = jnp.sum(weights.reshape(group // 8, 8, columns), axis=0)
+        mixed = lax.dot_general(
             slab,
             weights.astype(jnp.bfloat16),
             (((0,), (0,)), ((), ())),
             preferred_element_type=jnp.float32,
         )[HEAD_SIZE:]
-
-    def plain_step(step, carry):
-        slab, scores = scores_of(step)
-        weights = jnp.exp2(scores * LOG2E)
-        sum_ref[...] += jnp.sum(weights.reshape(block // 8, 8, columns), axis=0)
-        acc_ref[...] += weighed(slab, weights)
+        if guarded:
+            sum_ref[...] = sum_ref[...] * factor + added
+            acc_ref[...] = acc_ref[...] * factor + mixed
+        else:
+            sum_ref[...] += added
+            acc_ref[...] += mixed
         return carry
 
-    def guarded_step(step, carry):
-        slab, scores = scores_of(step)
-        before = max_ref[...]
-        top = jnp.maximum(before, jnp.max(scores, axis=0, keepdims=True))
-        factor = jnp.exp(before - top)
-        weights = jnp.exp(scores - top)
-        sum_ref[...] = sum_ref[...] * factor + jnp.sum(
-            weights.reshape(block // 8, 8, columns), axis=0
-        )
-        acc_ref[...] = acc_ref[...] * factor + weighed(slab, weights)
-        max_ref[...] = top
-        return carry
-
-    @pl.when(flag_ref[0] == 0)
-    def _():
-        lax.fori_loop(0, steps, plain_step, 0)
-
-    @pl.when(flag_ref[0] != 0)
-    def _():
-        max_ref[...] = jnp.full_like(max_ref, -1e30)
-        lax.fori_loop(0, steps, guarded_step, 0)
+    lax.fori_loop(0, 2 * Z_RING, step, 0)
 
     attended = acc_ref[...] / jnp.sum(sum_ref[...], axis=0, keepdims=True)
     mean_sq = jnp.mean(attended * attended, axis=0, keepdims=True)
     unit = attended * lax.rsqrt(mean_sq + EPS)
     turned = jnp.concatenate([unit, jnp.zeros_like(unit)], axis=0).T
-    tokens = out_ref.shape[0]
     low = lax.broadcasted_iota(jnp.int32, (tokens, 128), 1) < HEAD_SIZE
-    for pair in range(out_ref.shape[1] // 128):
+    for pair in range(mine_ref.shape[1] // 128):
         first = turned[(2 * pair) * tokens : (2 * pair + 1) * tokens, :]
         second = turned[(2 * pair + 1) * tokens : (2 * pair + 2) * tokens, :]
         joined = jnp.where(low, first, pltpu.roll(second, HEAD_SIZE, 1))
         lanes = slice(pair * 128, (pair + 1) * 128)
-        out_ref[:, lanes] = (joined * gain_ref[:, lanes]).astype(jnp.bfloat16)
+        mine_ref[:, lanes] = (joined * gain_ref[:, lanes]).astype(jnp.bfloat16)
+
+    part = tokens // tp_count
+
+    def rows_of(owner):
+        return mine_ref.at[pl.ds(pl.multiple_of((owner % tp_count) * part, part), part)]
+
+    def t_copy(r, source):
+        return remote(
+            rows_of(tp + r),
+            out_ref.at[source % tp_count],
+            t_send.at[r - 1],
+            t_recv.at[r - 1],
+            {"tp": (tp + r) % tp_count},
+        )
+
+    for r in range(1, tp_count):
+        t_copy(r, tp).start()
+    own = pltpu.make_async_copy(rows_of(tp), out_ref.at[tp], l_sem)
+    own.start()
+    own.wait()
+    for r in range(1, X_RING):
+        x_copy(r, x).wait_send()
+    for way in range(2):
+        for hop in range(Z_RING // 2):
+            z_out(way, hop).wait_send()
+    for number in range(Z_RING):
+        p_out(number).wait_send()
+    for r in range(1, tp_count):
+        t_copy(r, tp + tp_count - r).wait_recv()
+        t_copy(r, tp).wait_send()
 
 
 def dispatch_kernel(code_ref, normed_ref, out_ref):
@@ -318,25 +454,54 @@
             sine,
         ),
     )
-    gathered = lax.all_gather(packed, "sp", axis=0, tiled=True)
     codes = slot_codes(routes, tp_index, tp_count, sp_count)
     bound = 8.0 * jnp.max(jnp.abs(query_gain)) * jnp.max(jnp.abs(key_norm_gain))
-    wide = (bound > SAFE_BOUND).astype(jnp.int32)[None]
-    head_out = call(
-        functools.partial(attention_kernel, 1024),
-        shaped((tokens, heads * HEAD_SIZE)),
-        (wide, query_rows, gathered, head_gain[None]),
-        specs=[SM, VM, VM, VM],
-        scratch=(
-            pltpu.VMEM((HEAD_SIZE, columns), jnp.float32),
-            pltpu.VMEM((8, columns), jnp.float32),
-            pltpu.VMEM((1, columns), jnp.float32),
-        ),
-        flops=4 * columns * sequence_total * 128,
-        moved=sequence_total * 256,
-    )
     part_rows = tokens // tp_count
-    token_heads = lax.all_to_all(head_out, "tp", split_axis=0, concat_axis=1, tiled=True)
+
+    def attention(guarded, number):
+        def run(rows, own, gain):
+            return pl.pallas_call(
+                functools.partial(ring_attention_kernel, guarded),
+                out_shape=shaped((tp_count, part_rows, heads * HEAD_SIZE)),
+                in_specs=[VM, VM, VM],
+                out_specs=VM,
+                scratch_shapes=[
+                    pltpu.VMEM((Z_RING, 2, X_RING * tokens, 128), jnp.bfloat16),
+                    pltpu.VMEM((tokens, heads * HEAD_SIZE), jnp.bfloat16),
+                    pltpu.VMEM((HEAD_SIZE, columns), jnp.float32),
+                    pltpu.VMEM((8, columns), jnp.float32),
+                    pltpu.VMEM((1, columns), jnp.float32),
+                    pltpu.SemaphoreType.DMA((X_RING - 1,)),
+                    pltpu.SemaphoreType.DMA((X_RING - 1,)),
+                    pltpu.SemaphoreType.DMA((2, Z_RING // 2)),
+                    pltpu.SemaphoreType.DMA((2, Z_RING // 2)),
+                    pltpu.SemaphoreType.DMA((Z_RING,)),
+                    pltpu.SemaphoreType.DMA((Z_RING,)),
+                    pltpu.SemaphoreType.DMA((tp_count - 1,)),
+                    pltpu.SemaphoreType.DMA((tp_count - 1,)),
+                    pltpu.SemaphoreType.DMA,
+                ],
+                compiler_params=pltpu.CompilerParams(
+                    vmem_limit_bytes=56 * 2**20, collective_id=number, has_side_effects=True
+                ),
+                cost_estimate=pl.CostEstimate(
+                    flops=4 * columns * sequence_total * 128,
+                    bytes_accessed=sequence_total * 256,
+                    transcendentals=0,
+                ),
+            )(rows, own, gain)
+
+        return run
+
+    tiles = lax.cond(
+        bound > SAFE_BOUND,
+        attention(True, 1),
+        attention(False, 0),
+        query_rows,
+        packed,
+        head_gain[None],
+    )
+    token_heads = jnp.concatenate([tiles[t] for t in range(tp_count)], axis=1)
     own_resid = lax.dynamic_slice_in_dim(residual, tp_index * part_rows, part_rows, 0)
     hidden_own = (
         own_resid.astype(jnp.float32)

time: 375 us -> 290 us (0.77)
  waiting for transfers between devices: 157 us -> 72.7 us
  Pallas kernels: 75 us -> 90.8 us
  between operations: 14.9 us -> 1.44 us
  starting transfers between devices: 14.8 us -> 10.9 us
    all_gather x1 -> x0, waiting for transfers between devices: 77.4 us -> none  [local(): gathered = lax.all_gather(packed, 'sp', axis=0, tiled=True)]
    pallas_call x0 -> x1, Pallas kernels: none -> 65.9 us  [run(): pl.pallas_call(functools.partial(ring_attention_kernel, guarded), out_sha...]
    pallas_call x5 -> x4, Pallas kernels: 75 us -> 24.9 us  [call(): pl.pallas_call(kernel, out_shape=out_shape, in_specs=specs or [VM] * len(...]
    all_to_all x1 -> x0, waiting for transfers between devices: 5.86 us -> none  [local(): lax.all_to_all(head_out, 'tp', split_axis=0, concat_axis=1, tiled=True)]
    all_to_all x1 -> x0, starting transfers between devices: 4.29 us -> none  [local(): lax.all_to_all(head_out, 'tp', split_axis=0, concat_axis=1, tiled=True)]
  transfers between devices with their start and end apart: 4 -> 2, of which waited for: 4 -> 2; matrix products, arithmetic and copies ran while one was open for 2% -> 2% of each run, Pallas kernels for 0% -> 0%
where the time goes in v2:
time: 290 us; the launch traced here: 289 us
  blocking collectives  92 us (32%)
  Pallas kernels  90.8 us (31%)
  waiting for transfers between devices  72.7 us (25%)
  starting transfers between devices  10.9 us (4%)
  local copies, waits for them, and re-layouts  9.02 us (3%)
  other arithmetic  6.6 us (2%)
  matrix products  5.71 us (2%)
    all_to_all x1, blocking collectives, local(): lax.all_to_all(outgoing.reshape(sp_count, 8, wide_row), 'sp', split_axis=...  70.2 us
    pallas_call x1, Pallas kernels, run(): pl.pallas_call(functools.partial(ring_attention_kernel, guarded), out_sha...  65.9 us
    all_to_all x1, waiting for transfers between devices, local(): lax.all_to_all(produced.reshape(sp_count, 8, wide_row), 'sp', split_axis=...  59 us
    pallas_call x4, Pallas kernels, call(): pl.pallas_call(kernel, out_shape=out_shape, in_specs=specs or [VM] * len(...  24.9 us
    all_to_all x1, blocking collectives, sent_and_summed(): tiles = lax.all_to_all(split_up(value, dim, length), axis, 0, 0, tiled=True)  21.8 us
    all_to_all x1, waiting for transfers between devices, gather_rows(): lax.all_to_all(jnp.broadcast_to(value[None], (length, *value.shape)), axi...  13.6 us
    all_to_all x1, starting transfers between devices, local(): lax.all_to_all(produced.reshape(sp_count, 8, wide_row), 'sp', split_axis=...  7.02 us
  transfers between devices with their start and end apart: 2, of which 2 were waited for; matrix products, arithmetic and copies ran while one was open for 2% of the time, Pallas kernels for 0%

profile of v2, /device:TPU:32, one launch (start us, length us, event | category | flops | bytes accessed | tf_op | source)
XLA Modules:
  0.0 289.1 jit_solution(11351708772998962311)
XLA Ops:
  0.0 1.3 abs_reduce_fusion
  1.3 1.3 abs_reduce_fusion.1
  6.5 0.9 copy.29
  7.4 0.9 copy.30
  9.0 1.9 sine_multiply_fusion
  11.0 2.0 shard_map.163
  13.0 65.9 %conditional.1 = (bf16[4,80,256]{2,1,0:T(8,128)(2,1)S(1)}) conditional(s32[]{:T(128)} %convert_element_type.49, (bf16[1280,128]{1,0:T(8,128)(2,1)S(1)}, bf16[320,128]{1,0:T(8,128)(2,1)S(1)}, f32[1,256]{1,0:T(1,128)}) %tuple.38, (bf16[1280,128]{1,0:T(8,128)(2,1)S(1)}, bf16[320,128]{1,0:T(8,128)(2,1)S(1)}, f32[1,256]{1,0:T(1,128)}) %tuple.39), branch_computations={%region_2.3_spmd, %region_3.4_spmd} | conditional | flops 13421772800 | bytes 5242888 | solution.py:496
  13.0 65.9 %branch_1_fun.3 = bf16[4,80,256]{2,1,0:T(8,128)(2,1)S(1)} custom-call(bf16[1280,128]{1,0:T(8,128)(2,1)S(1)} %get-tuple-element.57.q_ref, bf16[320,128]{1,0:T(8,128)(2,1)S(1)} %get-tuple-element.58.packed_ref, f32[1,256]{1,0:T(1,128)} %get-tuple-element.59.gain_ref), custom_call_target="tpu_custom_call" | custom-call | flops 13421772800 | bytes 5242880 | tf_op jit(solution)/shard_map/cond/branch_1_fun/pallas_call | solution.py:463
  78.9 3.2 %multiply_reduce_fusion = (f32[80]{0:T(128)S(1)}, f32[80,2048]{1,0:T(8,128)S(1)}) fusion(bf16[1024,2048]{1,0:T(8,128)(2,1)} %param.25, bf16[80,256]{1,0:T(8,128)(2,1)S(1)} %get-tuple-element.65, bf16[80,256]{1,0:T(8,128)(2,1)S(1)} %get-tuple-element.66, bf16[80,256]{1,0:T(8,128)(2,1)S(1)} %get-tuple-element.67, bf16[80,256]{1,0:T(8,128)(2,1)S(1)} %get-tuple-element.64, ...), kind=kOutput, calls=%fused_computation.12 | convolution fusion | flops 337182656 | bytes 5341508 | tf_op jit(solution)/shard_map/dot_general | solution.py:508
  82.3 1.2 broadcast_in_dim.65
  83.5 3.9 %all-to-all-start = ((bf16[4,80,2048]{2,1,0:T(8,128)(2,1)}), bf16[4,80,2048]{2,1,0:T(8,128)(2,1)S(1)}, u32[]{:S(2)}, u32[]{:S(2)}) async-start(bf16[4,80,2048]{2,1,0:T(8,128)(2,1)} %broadcast_in_dim.65), calls=%async_computation | async-start | bytes 2621440 | tf_op jit(solution)/shard_map/all_to_all | solution.py:36
  87.9 0.8 fusion.4
  89.8 13.6 %all-to-all-done = bf16[4,80,2048]{2,1,0:T(8,128)(2,1)S(1)} async-done(((bf16[4,80,2048]{2,1,0:T(8,128)(2,1)}), bf16[4,80,2048]{2,1,0:T(8,128)(2,1)S(1)}, u32[]{:S(2)}, u32[]{:S(2)}) %all-to-all-start) | async-done | bytes 1310752 | tf_op jit(solution)/shard_map/all_to_all | solution.py:36
  103.5 1.2 copy-done.1
  104.6 5.6 %shard_map.164 = bf16[512,2560]{1,0:T(8,128)(2,1)} custom-call(s32[4,320]{1,0:T(4,128)} %copy.39.code_ref, bf16[320,2048]{1,0:T(8,128)(2,1)} %bitcast.24), custom_call_target="tpu_custom_call" | custom-call | flops 1342177280 | bytes 2621440 | tf_op jit(solution)/shard_map/pallas_call | solution.py:387
  110.2 70.2 %all_to_all.20 = bf16[64,8,2560]{2,1,0:T(8,128)(2,1)} all-to-all(bf16[64,8,2560]{2,1,0:T(8,128)(2,1)} %bitcast.28), channel_id=1, replica_groups=mesh['sp'=64,'tp'=4] {'sp'}, dimensions={0} | all-to-all | bytes 5242880 | tf_op jit(solution)/shard_map/all_to_all | solution.py:522
  180.4 10.6 %shard_map.165 = bf16[512,2560]{1,0:T(8,128)(2,1)} custom-call(bf16[512,2560]{1,0:T(8,128)(2,1)} %bitcast.29, bf16[2048,512]{1,0:T(8,128)(2,1)} %bitcast.32, bf16[2048,512]{1,0:T(8,128)(2,1)} %bitcast.33, bf16[512,2048]{1,0:T(8,128)(2,1)} %bitcast.34), custom_call_target="tpu_custom_call" | custom-call | flops 3221225472 | bytes 6291456 | tf_op jit(solution)/shard_map/pallas_call | solution.py:387
  191.0 7.0 %all-to-all-start.2 = ((bf16[64,8,2560]{2,1,0:T(8,128)(2,1)}), bf16[64,8,2560]{2,1,0:T(8,128)(2,1)}, u32[]{:S(2)}, u32[]{:S(2)}) async-start(bf16[64,8,2560]{2,1,0:T(8,128)(2,1)} %bitcast.27), calls=%async_computation.2 | async-start | bytes 5242880 | tf_op jit(solution)/shard_map/all_to_all | solution.py:537
  198.0 0.8 copy.40.weight_ref
  199.4 1.1 fusion.5.inner_ref
  200.5 59.0 %all-to-all-done.2 = bf16[64,8,2560]{2,1,0:T(8,128)(2,1)} async-done(((bf16[64,8,2560]{2,1,0:T(8,128)(2,1)}), bf16[64,8,2560]{2,1,0:T(8,128)(2,1)}, u32[]{:S(2)}, u32[]{:S(2)}) %all-to-all-start.2) | async-done | bytes 2621472 | tf_op jit(solution)/shard_map/all_to_all | solution.py:537
  259.6 6.8 %shard_map.166 = bf16[320,2048]{1,0:T(8,128)(2,1)} custom-call(s32[320,4]{1,0:T(8,128)} %copy-done.3, f32[320,4]{1,0:T(8,128)} %copy.40.weight_ref, bf16[512,2560]{1,0:T(8,128)(2,1)} %bitcast.13.back_ref, bf16[320,128]{1,0:T(8,128)(2,1)} %fusion.5.inner_ref, bf16[128,2048]{1,0:T(8,128)(2,1)} %down_ref.1), custom_call_target="tpu_custom_call" | custom-call | flops 1677721600 | bytes 2621440 | tf_op jit(solution)/shard_map/pallas_call | solution.py:387
  266.3 21.8 %all_to_all.21 = bf16[4,80,2048]{2,1,0:T(8,128)(2,1)S(1)} all-to-all(bf16[4,80,2048]{2,1,0:T(8,128)(2,1)} %bitcast.30), channel_id=1, replica_groups=mesh['sp'=64,'tp'=4] {'tp'}, dimensions={0} | all-to-all | bytes 2621440 | tf_op jit(solution)/shard_map/all_to_all | solution.py:30
  288.3 0.8 add_convert_fusion
  (41 shorter events, 5.8 us)
Async XLA Ops:
  0.0 198.9 %copy-start = (bf16[2048,128]{1,0:T(8,128)(2,1)S(1)}, bf16[2048,128]{1,0:T(8,128)(2,1)}, u32[]{:S(2)}) copy-start(bf16[2048,128]{1,0:T(8,128)(2,1)} %param.33) | copy-start | bytes 1572868
  78.9 3.3 %copy-start.5 = (f32[2048]{0:T(1024)S(1)}, f32[2048]{0:T(1024)}, u32[]{:S(2)}) copy-start(f32[2048]{0:T(1024)} %param.27) | copy-start | bytes 24580
  83.5 3.9 %copy-start.4 = (s32[320,4]{0,1:T(4,128)S(1)}, s32[320,4]{0,1:T(4,128)}, u32[]{:S(2)}) copy-start(s32[320,4]{0,1:T(4,128)} %param.28) | copy-start | bytes 15364
  83.5 20.0 %all-to-all-start = ((bf16[4,80,2048]{2,1,0:T(8,128)(2,1)}), bf16[4,80,2048]{2,1,0:T(8,128)(2,1)S(1)}, u32[]{:S(2)}, u32[]{:S(2)}) async-start(bf16[4,80,2048]{2,1,0:T(8,128)(2,1)} %broadcast_in_dim.65), calls=%async_computation | async-start | bytes 2621440 | tf_op jit(solution)/shard_map/all_to_all | solution.py:36
  89.1 21.1 %copy-start.3 = (s32[320,4]{1,0:T(8,128)}, s32[320,4]{1,0:T(8,128)S(1)}, u32[]{:S(2)}) copy-start(s32[320,4]{1,0:T(8,128)S(1)} %fusion.11.code_ref) | copy-start | bytes 15364
  103.5 1.2 copy-start.1
  191.0 7.0 %copy-start.6 = (f32[320,4]{0,1:T(4,128)S(1)}, f32[320,4]{0,1:T(4,128)}, u32[]{:S(2)}) copy-start(f32[320,4]{0,1:T(4,128)} %param.29) | copy-start | bytes 15364
  191.0 7.9 %copy-start.2 = (bf16[4,80,2048]{2,1,0:T(8,128)(2,1)S(1)}, bf16[4,80,2048]{2,1,0:T(8,128)(2,1)}, u32[]{:S(2)}) copy-start(bf16[4,80,2048]{2,1,0:T(8,128)(2,1)} %copy-done.1) | copy-start | bytes 3932164
  191.0 68.6 %all-to-all-start.2 = ((bf16[64,8,2560]{2,1,0:T(8,128)(2,1)}), bf16[64,8,2560]{2,1,0:T(8,128)(2,1)}, u32[]{:S(2)}, u32[]{:S(2)}) async-start(bf16[64,8,2560]{2,1,0:T(8,128)(2,1)} %bitcast.27), calls=%async_computation.2 | async-start | bytes 5242880 | tf_op jit(solution)/shard_map/all_to_all | solution.py:537
  198.0 1.3 copy-start.7

commit v3 on v2

--- a/solution.py
+++ b/solution.py
@@ -16,27 +16,7 @@
 SAFE_BOUND = 70.0
 
 VM = pl.BlockSpec(memory_space=pltpu.VMEM)
-SM = pl.BlockSpec(memory_space=pltpu.SMEM)
-
-
-def split_up(value, dim, length):
-    dims = value.shape
-    tiles = value.reshape(*dims[:dim], length, dims[dim] // length, *dims[dim + 1 :])
-    return jnp.moveaxis(tiles, dim, 0)
-
-
-def sent_and_summed(value, axis, dim):
-    length = lax.axis_size(axis)
-    tiles = lax.all_to_all(split_up(value, dim, length), axis, 0, 0, tiled=True)
-    return jnp.sum(tiles.astype(jnp.float32), axis=0)
-
-
-def gather_rows(value, axis):
-    length = lax.axis_size(axis)
-    tiles = lax.all_to_all(
-        jnp.broadcast_to(value[None], (length, *value.shape)), axis, 0, 0, tiled=True
-    )
-    return tiles.reshape(length * value.shape[0], value.shape[1])
+ANY = pl.BlockSpec(memory_space=pl.ANY)
 
 
 def final_norm(field, gain):
@@ -91,6 +71,7 @@
 
 MESH = pl.DeviceIdType.MESH
 Z_RING, X_RING = 8, 4
+PLANE = 2 * X_RING
 
 
 def ring_attention_kernel(
@@ -289,98 +270,367 @@
         t_copy(r, tp).wait_send()
 
 
-def dispatch_kernel(code_ref, normed_ref, out_ref):
-    tokens, width = normed_ref.shape
-    rows = out_ref.shape[0]
+def moe_kernel(
+    heads_ref,
+    out_proj_ref,
+    residual_ref,
+    ffn_gain_ref,
+    code_ref,
+    code_t_ref,
+    weight_ref,
+    shared_gate_ref,
+    shared_up_ref,
+    shared_down_ref,
+    gate_hbm,
+    up_hbm,
+    down_hbm,
+    out_ref,
+    own_ref,
+    hidden_ref,
+    normed_ref,
+    leaving_ref,
+    passing_ref,
+    arrived_ref,
+    made_ref,
+    back_passing_ref,
+    back_ref,
+    acc_ref,
+    part_ref,
+    got_ref,
+    gate_ref,
+    up_ref,
+    down_ref,
+    w_sem,
+    l_sem,
+    y_send,
+    y_recv,
+    s_send,
+    s_recv,
+    z_send,
+    z_recv,
+    i_send,
+    i_recv,
+    i_local,
+    bz_send,
+    bz_recv,
+    bi_send,
+    bi_recv,
+    bi_local,
+):
+    sp, tp = lax.axis_index("sp"), lax.axis_index("tp")
+    tp_count = lax.axis_size("tp")
+    z, i = sp // PLANE, sp % PLANE
+    part, width = hidden_ref.shape
+    tokens = part * tp_count
     quarter = width // 4
-    row = lax.broadcasted_iota(jnp.int32, (rows, tokens), 0)
-    main_code = (row // 8) * 16 + row % 8
-    extra_code = (row // 8) * 16 + 8 + (row % 8) // 4
-    main = jnp.zeros((rows, tokens), jnp.float32)
-    extra = jnp.zeros((rows, tokens), jnp.float32)
-    for k in range(code_ref.shape[0]):
-        own = code_ref[k : k + 1, :]
-        main += jnp.where(main_code == own, 1.0, 0.0)
-        extra += jnp.where(extra_code == own, 1.0, 0.0)
-    main = main.astype(jnp.bfloat16)
-    for q in range(4):
-        cols = slice(q * quarter, (q + 1) * quarter)
-        out_ref[:, cols] = jnp.dot(
-            main, normed_ref[:, cols], preferred_element_type=jnp.float32
-        ).astype(jnp.bfloat16)
-    total = jnp.zeros((rows, quarter), jnp.float32)
-    for q in range(4):
-        part = jnp.where(row % 4 == q, extra, 0.0).astype(jnp.bfloat16)
+    rows = PLANE * 8
+    top = code_ref.shape[1]
+
+    def at_z(z_at):
+        return {"sp": (z_at % Z_RING) * PLANE + i}
+
+    def at_i(i_at):
+        return {"sp": z * PLANE + i_at % PLANE}
+
+    def at_tp(t):
+        return {"tp": t % tp_count}
+
+    barrier = pltpu.get_barrier_semaphore()
+    others = [at_z(z + k) for k in range(1, Z_RING)]
+    others += [at_i(i + r) for r in range(1, PLANE)]
+    others += [at_tp(tp + r) for r in range(1, tp_count)]
+    for other in others:
+        pl.semaphore_signal(barrier, inc=1, device_id=other, device_id_type=MESH)
+
+    loads = [
+        pltpu.make_async_copy(
+            residual_ref.at[pl.ds(pl.multiple_of(tp * part, part), part)], own_ref, l_sem
+        ),
+        pltpu.make_async_copy(gate_hbm, gate_ref, w_sem.at[0]),
+        pltpu.make_async_copy(up_hbm, up_ref, w_sem.at[1]),
+        pltpu.make_async_copy(down_hbm, down_ref, w_sem.at[2]),
+    ]
+    for load in loads:
+        load.start()
+
+    def remote(src, dst, send_sem, recv_sem, to):
+        return pltpu.make_async_remote_copy(
+            src_ref=src,
+            dst_ref=dst,
+            send_sem=send_sem,
+            recv_sem=recv_sem,
+            device_id=to,
+            device_id_type=MESH,
+        )
+
+    loads[0].wait()
+    size = heads_ref.shape[2]
+    total = own_ref[...].astype(jnp.float32)
+    for t in range(tp_count):
         total += jnp.dot(
-            part,
-            normed_ref[:, q * quarter : (q + 1) * quarter],
+            heads_ref[t],
+            out_proj_ref[t * size : (t + 1) * size, :],
             preferred_element_type=jnp.float32,
         )
-    out_ref[:, width:] = total.astype(jnp.bfloat16)
-
-
-def expert_kernel(in_ref, gate_ref, up_ref, down_ref, out_ref, rows_ref, inner_ref):
-    rows = in_ref.shape[0]
-    width = gate_ref.shape[0]
-    quarter = width // 4
-    extra_rows = rows // 4
-    rows_ref[:rows, :] = in_ref[:, :width]
-    tail = in_ref[:, width:]
-    place = lax.broadcasted_iota(jnp.int32, (extra_rows, rows), 1)
-    index = lax.broadcasted_iota(jnp.int32, (extra_rows, rows), 0)
-    for q in range(4):
-        pick = jnp.where(place == 4 * index + q, 1.0, 0.0).astype(jnp.bfloat16)
-        rows_ref[rows:, q * quarter : (q + 1) * quarter] = jnp.dot(
-            pick, tail, preferred_element_type=jnp.float32
-        ).astype(jnp.bfloat16)
-    every = rows_ref[...]
-    gate = jnp.dot(every, gate_ref[...], preferred_element_type=jnp.float32)
-    up = jnp.dot(every, up_ref[...], preferred_element_type=jnp.float32)
-    inner_ref[...] = (gate / (1.0 + jnp.exp(-gate)) * up).astype(jnp.bfloat16)
-    place = lax.broadcasted_iota(jnp.int32, (rows, extra_rows), 0)
-    index = lax.broadcasted_iota(jnp.int32, (rows, extra_rows), 1)
-    total = jnp.zeros((rows, quarter), jnp.float32)
-    for q in range(4):
-        cols = slice(q * quarter, (q + 1) * quarter)
-        made = jnp.dot(
-            inner_ref[...], down_ref[:, cols], preferred_element_type=jnp.float32
-        ).astype(jnp.bfloat16)
-        out_ref[:, cols] = made[:rows]
-        pick = jnp.where(place == 4 * index + q, 1.0, 0.0).astype(jnp.bfloat16)
-        total += jnp.dot(pick, made[rows:], preferred_element_type=jnp.float32)
-    out_ref[:, width:] = total.astype(jnp.bfloat16)
-
-
-def combine_kernel(code_ref, weight_ref, back_ref, inner_ref, down_ref, out_ref):
-    tokens, width = out_ref.shape
-    rows = back_ref.shape[0]
-    quarter = width // 4
-    place = lax.broadcasted_iota(jnp.int32, (tokens, rows), 1)
-    main_code = (place // 8) * 16 + place % 8
-    extra_code = (place // 8) * 16 + 8 + (place % 8) // 4
-    main = jnp.zeros((tokens, rows), jnp.float32)
-    extra = jnp.zeros((tokens, rows), jnp.float32)
-    for k in range(code_ref.shape[1]):
-        own = code_ref[:, k : k + 1]
-        scale = weight_ref[:, k : k + 1]
-        main += jnp.where(main_code == own, scale, 0.0)
-        extra += jnp.where(extra_code == own, scale, 0.0)
-
-    def parts_of(value):
-        high = value.astype(jnp.bfloat16)
-        return high, (value - high.astype(jnp.float32)).astype(jnp.bfloat16)
-
-    high, low = parts_of(main)
-    tail = back_ref[:, width:]
-    for q in range(4):
-        cols = slice(q * quarter, (q + 1) * quarter)
-        own_high, own_low = parts_of(jnp.where(place % 4 == q, extra, 0.0))
-        total = jnp.dot(inner_ref[...], down_ref[:, cols], preferred_element_type=jnp.float32)
-        total += jnp.dot(high, back_ref[:, cols], preferred_element_type=jnp.float32)
-        total += jnp.dot(low, back_ref[:, cols], preferred_element_type=jnp.float32)
-        total += jnp.dot(own_high, tail, preferred_element_type=jnp.float32)
-        total += jnp.dot(own_low, tail, preferred_element_type=jnp.float32)
-        out_ref[:, cols] = total.astype(jnp.bfloat16)
+    hidden = total.astype(jnp.bfloat16).astype(jnp.float32)
+    hidden_ref[...] = hidden
+    normed_ref[tp] = final_norm(hidden, ffn_gain_ref[...]).astype(jnp.bfloat16)
+    pl.semaphore_wait(barrier, len(others))
+
+    def y_copy(r, source):
+        return remote(
+            normed_ref.at[source % tp_count],
+            normed_ref.at[source % tp_count],
+            y_send.at[r - 1],
+            y_recv.at[r - 1],
+            at_tp(tp + r),
+        )
+
+    for r in (2, 1, 3):
+        y_copy(r, tp).start()
+    for r in range(1, tp_count):
+        y_copy(r, tp + tp_count - r).wait_recv()
+
+    def turn(n):
+        odd = n % 2
+        return odd * ((n + 1) // 2) + (1 - odd) * ((Z_RING - n // 2) % Z_RING)
+
+    def z_copy(k, z_from, z_to):
+        return remote(
+            leaving_ref.at[z_to % Z_RING],
+            passing_ref.at[z_from % Z_RING],
+            z_send.at[k],
+            z_recv.at[k],
+            at_z(z + k),
+        )
+
+    def bz_copy(k, z_from, z_to):
+        return remote(
+            made_ref.at[z_to % Z_RING],
+            back_passing_ref.at[z_from % Z_RING],
+            bz_send.at[k],
+            bz_recv.at[k],
+            at_z(z + Z_RING - k),
+        )
+
+    def i_copy(source_ref, target_ref, sends, recvs, k, z_at, r, tile, place):
+        return remote(
+            source_ref.at[z_at % Z_RING, tile % PLANE],
+            target_ref.at[z_at % Z_RING, place % PLANE],
+            sends.at[k, r - 1],
+            recvs.at[k, r - 1],
+            at_i(i + r),
+        )
+
+    def spread(source_ref, target_ref, sends, recvs, locals_, k, z_at):
+        for r in range(1, PLANE):
+            i_copy(source_ref, target_ref, sends, recvs, k, z_at, r, i + r, i).start()
+        pltpu.make_async_copy(
+            source_ref.at[z_at % Z_RING, i], target_ref.at[z_at % Z_RING, i], locals_.at[k]
+        ).start()
+
+    def collected(source_ref, target_ref, sends, recvs, locals_, k, z_at):
+        for r in range(1, PLANE):
+            place = i + PLANE - r
+            i_copy(source_ref, target_ref, sends, recvs, k, z_at, r, i, place).wait_recv()
+        pltpu.make_async_copy(
+            source_ref.at[z_at % Z_RING, i], target_ref.at[z_at % Z_RING, i], locals_.at[k]
+        ).wait()
+
+    def sent(source_ref, target_ref, sends, recvs, k, z_at):
+        for r in range(1, PLANE):
+            i_copy(source_ref, target_ref, sends, recvs, k, z_at, r, i + r, i).wait_send()
+
+    def dispatch(n, carry):
+        k = turn(n)
+        z_to = (z + k) % Z_RING
+        row = lax.broadcasted_iota(jnp.int32, (rows, tokens), 0)
+        base = (z_to * PLANE + row // 8) * 16
+        main_code = base + row % 8
+        extra_code = base + 8 + (row % 8) // 4
+        main = jnp.zeros((rows, tokens), jnp.float32)
+        extra = jnp.zeros((rows, tokens), jnp.float32)
+        for slot in range(top):
+            own = code_t_ref[slot : slot + 1, :]
+            main += jnp.where(main_code == own, 1.0, 0.0)
+            extra += jnp.where(extra_code == own, 1.0, 0.0)
+        main = main.astype(jnp.bfloat16)
+        normed = normed_ref[...].reshape(tokens, width)
+        tail = jnp.zeros((rows, quarter), jnp.float32)
+        for q in range(4):
+            cols = slice(q * quarter, (q + 1) * quarter)
+            leaving_ref[z_to, :, :, cols] = (
+                jnp.dot(main, normed[:, cols], preferred_element_type=jnp.float32)
+                .astype(jnp.bfloat16)
+                .reshape(PLANE, 8, quarter)
+            )
+            chosen = jnp.where(row % 4 == q, extra, 0.0).astype(jnp.bfloat16)
+            tail += jnp.dot(chosen, normed[:, cols], preferred_element_type=jnp.float32)
+        leaving_ref[z_to, :, :, width:] = tail.astype(jnp.bfloat16).reshape(PLANE, 8, quarter)
+
+        @pl.when(n == 0)
+        def _():
+            spread(leaving_ref, arrived_ref, i_send, i_recv, i_local, 0, z)
+
+        @pl.when(n > 0)
+        def _():
+            z_copy(k, z, z + k).start()
+
+        return carry
+
+    lax.fori_loop(0, Z_RING, dispatch, 0)
+
+    normed = normed_ref[...].reshape(tokens, width)
+    gate = jnp.dot(normed, shared_gate_ref[...], preferred_element_type=jnp.float32)
+    up = jnp.dot(normed, shared_up_ref[...], preferred_element_type=jnp.float32)
+    inner = (gate / (1.0 + jnp.exp(-gate)) * up).astype(jnp.bfloat16)
+    acc_ref[...] = jnp.dot(inner, shared_down_ref[...], preferred_element_type=jnp.float32)
+    for load in loads[1:]:
+        load.wait()
+
+    def expert(k):
+        z_from = (z + Z_RING - k) % Z_RING
+        tiles = arrived_ref[z_from].reshape(rows, width + quarter)
+        extra_rows = rows // 4
+        place = lax.broadcasted_iota(jnp.int32, (extra_rows, rows), 1)
+        index = lax.broadcasted_iota(jnp.int32, (extra_rows, rows), 0)
+        pieces = []
+        for q in range(4):
+            pick = jnp.where(place == 4 * index + q, 1.0, 0.0).astype(jnp.bfloat16)
+            pieces.append(
+                jnp.dot(pick, tiles[:, width:], preferred_element_type=jnp.float32).astype(
+                    jnp.bfloat16
+                )
+            )
+        every = jnp.concatenate([tiles[:, :width], jnp.concatenate(pieces, axis=1)], axis=0)
+        gate = jnp.dot(every, gate_ref[...], preferred_element_type=jnp.float32)
+        up = jnp.dot(every, up_ref[...], preferred_element_type=jnp.float32)
+        inner = (gate / (1.0 + jnp.exp(-gate)) * up).astype(jnp.bfloat16)
+        place = lax.broadcasted_iota(jnp.int32, (rows, extra_rows), 0)
+        index = lax.broadcasted_iota(jnp.int32, (rows, extra_rows), 1)
+        tail = jnp.zeros((rows, quarter), jnp.float32)
+        for q in range(4):
+            cols = slice(q * quarter, (q + 1) * quarter)
+            made = jnp.dot(inner, down_ref[:, cols], preferred_element_type=jnp.float32).astype(
+                jnp.bfloat16
+            )
+            made_ref[z_from, :, :, cols] = made[:rows].reshape(PLANE, 8, quarter)
+            pick = jnp.where(place == 4 * index + q, 1.0, 0.0).astype(jnp.bfloat16)
+            tail += jnp.dot(pick, made[rows:], preferred_element_type=jnp.float32)
+        made_ref[z_from, :, :, width:] = tail.astype(jnp.bfloat16).reshape(PLANE, 8, quarter)
+
+    def arrivals(n, carry):
+        @pl.when((n > 0) & (n < Z_RING))
+        def _():
+            k = turn(n)
+            z_copy(k, z + Z_RING - k, z).wait_recv()
+            spread(passing_ref, arrived_ref, i_send, i_recv, i_local, k, z + Z_RING - k)
+
+        @pl.when(n > 0)
+        def _():
+            k = turn(n - 1)
+            collected(
+                passing_ref, arrived_ref, i_send, i_recv, i_local, k, z + Z_RING - k
+            )
+            expert(k)
+
+            @pl.when(n > 1)
+            def _():
+                bz_copy(k, z, z + Z_RING - k).start()
+
+            @pl.when(n == 1)
+            def _():
+                spread(made_ref, back_ref, bi_send, bi_recv, bi_local, 0, z)
+
+        return carry
+
+    lax.fori_loop(0, Z_RING + 1, arrivals, 0)
+
+    def combine(z_at):
+        tiles = back_ref[z_at].reshape(rows, width + quarter)
+        twice = jnp.concatenate([tiles, tiles], axis=0)
+        lane = lax.broadcasted_iota(jnp.int32, (tokens, 2 * rows), 1)
+        place = lane % rows
+        base = (z_at * PLANE + place // 8) * 16
+        main_code = base + place % 8
+        extra_code = base + 8 + (place % 8) // 4
+        main = jnp.zeros((tokens, 2 * rows), jnp.float32)
+        extra = jnp.zeros((tokens, 2 * rows), jnp.float32)
+        for slot in range(top):
+            own = code_ref[:, slot : slot + 1]
+            scale = weight_ref[:, slot : slot + 1]
+            main += jnp.where(main_code == own, scale, 0.0)
+            extra += jnp.where(extra_code == own, scale, 0.0)
+
+        def two_terms(value):
+            high = value.astype(jnp.bfloat16).astype(jnp.float32)
+            return jnp.where(lane < rows, high, value - high)
+
+        main, extra = two_terms(main), two_terms(extra)
+        main = main.astype(jnp.bfloat16)
+        for q in range(4):
+            cols = slice(q * quarter, (q + 1) * quarter)
+            chosen = jnp.where(place % 4 == q, extra, 0.0).astype(jnp.bfloat16)
+            acc_ref[:, cols] += jnp.dot(
+                main, twice[:, cols], preferred_element_type=jnp.float32
+            ) + jnp.dot(chosen, twice[:, width:], preferred_element_type=jnp.float32)
+
+    def returns(n, carry):
+        @pl.when((n > 0) & (n < Z_RING))
+        def _():
+            k = turn(n)
+            bz_copy(k, z + k, z).wait_recv()
+            spread(back_passing_ref, back_ref, bi_send, bi_recv, bi_local, k, z + k)
+
+        @pl.when(n > 0)
+        def _():
+            k = turn(n - 1)
+            collected(back_passing_ref, back_ref, bi_send, bi_recv, bi_local, k, z + k)
+            combine((z + k) % Z_RING)
+
+        return carry
+
+    lax.fori_loop(0, Z_RING + 1, returns, 0)
+
+    def s_copy(r, source):
+        return remote(
+            part_ref.at[(tp + r) % tp_count],
+            got_ref.at[source % tp_count],
+            s_send.at[r - 1],
+            s_recv.at[r - 1],
+            at_tp(tp + r),
+        )
+
+    for r in (2, 1, 3, 0):
+        owner = (tp + r) % tp_count
+        own_rows = pl.ds(pl.multiple_of(owner * part, part), part)
+        part_ref[owner] = acc_ref[own_rows, :].astype(jnp.bfloat16)
+        if r:
+            s_copy(r, tp).start()
+        else:
+            got_ref[tp] = part_ref[tp]
+    for r in range(1, tp_count):
+        s_copy(r, tp + tp_count - r).wait_recv()
+    total = hidden_ref[...]
+    for t in range(tp_count):
+        total += got_ref[t].astype(jnp.float32)
+    out_ref[...] = total.astype(jnp.bfloat16)
+
+    for r in range(1, tp_count):
+        y_copy(r, tp).wait_send()
+        s_copy(r, tp).wait_send()
+
+    def drain(n, carry):
+        @pl.when(n > 0)
+        def _():
+            z_copy(n, z, z + n).wait_send()
+            bz_copy(n, z, z + Z_RING - n).wait_send()
+
+        sent(passing_ref, arrived_ref, i_send, i_recv, n, z + Z_RING - n)
+        sent(back_passing_ref, back_ref, bi_send, bi_recv, n, z + n)
+        return carry
+
+    lax.fori_loop(0, Z_RING, drain, 0)
 
 
 def call(kernel, out_shape, args, specs=None, scratch=(), flops=0, moved=0):
@@ -501,54 +751,67 @@
         packed,
         head_gain[None],
     )
-    token_heads = jnp.concatenate([tiles[t] for t in range(tp_count)], axis=1)
-    own_resid = lax.dynamic_slice_in_dim(residual, tp_index * part_rows, part_rows, 0)
-    hidden_own = (
-        own_resid.astype(jnp.float32)
-        + jnp.dot(token_heads, out_proj, preferred_element_type=jnp.float32)
-    ).astype(jnp.bfloat16)
-    normed_own = final_norm(hidden_own.astype(jnp.float32), ffn_gain).astype(jnp.bfloat16)
-    normed = gather_rows(normed_own, "tp")
-    width = normed.shape[1]
-    rows = sp_count * 8
+    width = residual.shape[1]
+    hidden_units = expert_gate.shape[2]
     wide_row = width + width // 4
-    outgoing = call(
-        dispatch_kernel,
-        shaped((rows, wide_row)),
-        (codes.T, normed),
-        flops=4 * rows * tokens * width,
-        moved=rows * wide_row * 2,
+    tile_set = pltpu.VMEM((Z_RING, PLANE, 8, wide_row), jnp.bfloat16)
+    dma = pltpu.SemaphoreType.DMA
+    return pl.pallas_call(
+        moe_kernel,
+        out_shape=shaped((part_rows, width)),
+        in_specs=[VM, VM, ANY] + [VM] * 7 + [ANY] * 3,
+        out_specs=VM,
+        scratch_shapes=[
+            pltpu.VMEM((part_rows, width), jnp.bfloat16),
+            pltpu.VMEM((part_rows, width), jnp.float32),
+            pltpu.VMEM((tp_count, part_rows, width), jnp.bfloat16),
+            tile_set,
+            tile_set,
+            tile_set,
+            tile_set,
+            tile_set,
+            tile_set,
+            pltpu.VMEM((tokens, width), jnp.float32),
+            pltpu.VMEM((tp_count, part_rows, width), jnp.bfloat16),
+            pltpu.VMEM((tp_count, part_rows, width), jnp.bfloat16),
+            pltpu.VMEM((width, hidden_units), jnp.bfloat16),
+            pltpu.VMEM((width, hidden_units), jnp.bfloat16),
+            pltpu.VMEM((hidden_units, width), jnp.bfloat16),
+            dma((3,)),
+            dma,
+            dma((tp_count - 1,)),
+            dma((tp_count - 1,)),
+            dma((tp_count - 1,)),
+            dma((tp_count - 1,)),
+            dma((Z_RING,)),
+            dma((Z_RING,)),
+            dma((Z_RING, PLANE - 1)),
+            dma((Z_RING, PLANE - 1)),
+            dma((Z_RING,)),
+            dma((Z_RING,)),
+            dma((Z_RING,)),
+            dma((Z_RING, PLANE - 1)),
+            dma((Z_RING, PLANE - 1)),
+            dma((Z_RING,)),
+        ],
+        compiler_params=pltpu.CompilerParams(
+            vmem_limit_bytes=58 * 2**20, collective_id=2, has_side_effects=True
+        ),
+    )(
+        tiles,
+        out_proj,
+        residual,
+        ffn_gain[None],
+        codes,
+        codes.T,
+        route_weights,
+        shared_gate,
+        shared_up,
+        shared_down,
+        expert_gate[0],
+        expert_up[0],
+        expert_down[0],
     )
-    arrived = lax.all_to_all(
-        outgoing.reshape(sp_count, 8, wide_row), "sp", split_axis=0, concat_axis=0, tiled=True
-    )
-    hidden_units = expert_gate.shape[2]
-    produced = call(
-        expert_kernel,
-        shaped((rows, wide_row)),
-        (arrived.reshape(rows, wide_row), expert_gate[0], expert_up[0], expert_down[0]),
-        scratch=(
-            pltpu.VMEM((rows + rows // 4, width), jnp.bfloat16),
-            pltpu.VMEM((rows + rows // 4, hidden_units), jnp.bfloat16),
-        ),
-        flops=6 * rows * width * hidden_units,
-        moved=3 * width * hidden_units * 2,
-    )
-    returned = lax.all_to_all(
-        produced.reshape(sp_count, 8, wide_row), "sp", split_axis=0, concat_axis=0, tiled=True
-    ).reshape(rows, wide_row)
-    gate_part = jnp.dot(normed, shared_gate, preferred_element_type=jnp.float32)
-    up_part = jnp.dot(normed, shared_up, preferred_element_type=jnp.float32)
-    shared_inner = (jax.nn.silu(gate_part) * up_part).astype(jnp.bfloat16)
-    partial = call(
-        combine_kernel,
-        shaped((tokens, width)),
-        (codes, route_weights, returned, shared_inner, shared_down),
-        flops=5 * tokens * rows * width,
-        moved=rows * wide_row * 2,
-    )
-    mixed = sent_and_summed(partial, "tp", 0)
-    return (hidden_own.astype(jnp.float32) + mixed).astype(jnp.bfloat16)
 
 
 def solution(mesh):

time: 290 us -> 256 us (0.88)
  the two profiles are of different devices: /device:TPU:32 before, /device:TPU:161 now
where the time goes in v3:
time: 256 us; the launch traced here: 255 us
  Pallas kernels  239 us (93%)
  local copies, waits for them, and re-layouts  8.37 us (3%)
  other arithmetic  5.29 us (2%)
    pallas_call x1, Pallas kernels, local(): pl.pallas_call(moe_kernel, out_shape=shaped((part_rows, width)), in_specs...  177 us
    pallas_call x1, Pallas kernels, run(): pl.pallas_call(functools.partial(ring_attention_kernel, guarded), out_sha...  60.3 us

profile of v3, /device:TPU:161, one launch (start us, length us, event | category | flops | bytes accessed | tf_op | source)
XLA Modules:
  0.0 255.3 jit_solution(2152707108727690472)
XLA Ops:
  0.0 0.1 mul.33
  0.1 1.9 sine_multiply_fusion
  2.1 0.9 copy.22
  3.0 0.9 copy.23
  3.9 0.7 pad_maximum_fusion.kv_ref
  4.6 0.7 tile.6
  5.3 0.7 broadcast_in_dim_tile.7.qg_ref
  5.9 0.7 tile.7
  6.6 0.6 broadcast_in_dim_tile.8.kg_ref
  7.2 2.0 shard_map.163
  9.2 1.3 abs_reduce_fusion.1
  11.1 1.3 abs_reduce_fusion
  13.1 0.0 copy-start.1
  13.1 60.5 %conditional.1 = (bf16[4,80,256]{2,1,0:T(8,128)(2,1)S(1)}) conditional(s32[]{:T(128)} %convert_element_type.26, (bf16[1280,128]{1,0:T(8,128)(2,1)S(1)}, bf16[320,128]{1,0:T(8,128)(2,1)S(1)}, f32[1,256]{1,0:T(1,128)}) %tuple.16, (bf16[1280,128]{1,0:T(8,128)(2,1)S(1)}, bf16[320,128]{1,0:T(8,128)(2,1)S(1)}, f32[1,256]{1,0:T(1,128)}) %tuple.17), branch_computations={%region_2.3_spmd, %region_3.4_spmd} | conditional | flops 13421772800 | bytes 5242888 | solution.py:746
  13.1 60.3 %branch_1_fun.1 = bf16[4,80,256]{2,1,0:T(8,128)(2,1)S(1)} custom-call(bf16[1280,128]{1,0:T(8,128)(2,1)S(1)} %get-tuple-element.23.q_ref, bf16[320,128]{1,0:T(8,128)(2,1)S(1)} %get-tuple-element.24.packed_ref, f32[1,256]{1,0:T(1,128)} %get-tuple-element.25.gain_ref), custom_call_target="tpu_custom_call" | custom-call | flops 13421772800 | bytes 5242880 | tf_op jit(solution)/shard_map/cond/branch_1_fun/pallas_call | solution.py:713
  73.6 0.1 copy.24
  73.8 0.1 reshape.122
  74.0 0.8 fusion.2
  74.8 0.2 convert_element_type.30
  75.0 0.1 copy.25
  75.1 0.8 copy.26.code_ref
  76.0 0.8 copy.27.weight_ref
  76.8 176.8 %shard_map.164 = bf16[80,2048]{1,0:T(8,128)(2,1)} custom-call(bf16[4,80,256]{2,1,0:T(8,128)(2,1)S(1)} %get-tuple-element.34.heads_ref, bf16[1024,2048]{1,0:T(8,128)(2,1)} %out_proj_ref.1, bf16[320,2048]{1,0:T(8,128)(2,1)} %residual_ref.1, f32[1,2048]{1,0:T(1,128)} %bitcast.10, s32[320,4]{1,0:T(8,128)} %copy.26.code_ref, s32[4,320]{1,0:T(4,128)} %bitcast.9, ...), custom_call_target="tpu_custom_call" | custom-call | tf_op jit(solution)/shard_map/pallas_call | solution.py:759
  253.6 1.7 copy.31
  (14 shorter events, 0.1 us)
Async XLA Ops:
  13.1 60.6 %copy-start.1 = (s32[320,4]{0,1:T(4,128)S(1)}, s32[320,4]{0,1:T(4,128)}, u32[]{:S(2)}) copy-start(s32[320,4]{0,1:T(4,128)} %param.28) | copy-start | bytes 15364
  74.0 2.0 copy-start.2
  75.1 1.6 copy-start

commit v4 on v3

--- a/solution.py
+++ b/solution.py
@@ -12,7 +12,6 @@
 EPS = 1e-06
 THETA = 10000.0
 LOG2E = 1.4426950408889634
-CAPACITY = 10
 SAFE_BOUND = 70.0
 
 VM = pl.BlockSpec(memory_space=pltpu.VMEM)
@@ -52,16 +51,25 @@
     return unit * cosine + partner * sine
 
 
-def prepare_kernel(q_ref, kv_ref, qg_ref, kg_ref, cos_ref, sin_ref, rows_ref, packed_ref):
+def prepare_kernel(
+    q_ref, key_ref, value_ref, qg_ref, kg_ref, cos_ref, sin_ref, rows_ref, packed_ref, bound_ref
+):
     tokens = q_ref.shape[0]
     cosine, sine = cos_ref[...], sin_ref[...]
     low = lax.broadcasted_iota(jnp.int32, (tokens, 128), 1) < HEAD_SIZE
-    both = kv_ref[...].astype(jnp.float32)
-    turned = normed_and_turned(both, kg_ref[...], cosine, sine)
+    query_gain = jnp.concatenate([qg_ref[...], qg_ref[...]], axis=1)
+    key_gain = jnp.concatenate([kg_ref[...], kg_ref[...]], axis=1)
+    top = jnp.max(jnp.abs(query_gain), axis=1, keepdims=True)
+    top = top * jnp.max(jnp.abs(key_gain), axis=1, keepdims=True) * (HEAD_SIZE**0.5)
+    bound_ref[...] = jnp.broadcast_to(top, bound_ref.shape)
+    both = jnp.concatenate(
+        [key_ref[...].astype(jnp.float32), value_ref[...].astype(jnp.float32)], axis=0
+    ).T
+    turned = normed_and_turned(both, key_gain, cosine, sine)
     packed_ref[...] = jnp.where(low, turned, both).astype(jnp.bfloat16)
     for pair in range(q_ref.shape[1] // 128):
         field = q_ref[:, pair * 128 : (pair + 1) * 128].astype(jnp.float32)
-        turned = normed_and_turned(field, qg_ref[...], cosine, sine).astype(jnp.bfloat16)
+        turned = normed_and_turned(field, query_gain, cosine, sine).astype(jnp.bfloat16)
         turned = turned.astype(jnp.float32) * (HEAD_SIZE**-0.5)
         first = jnp.where(low, turned, 0.0)
         second = jnp.where(low, pltpu.roll(turned, HEAD_SIZE, 1), 0.0)
@@ -89,6 +97,10 @@
     x_recv,
     z_send,
     z_recv,
+    v_send,
+    v_recv,
+    u_send,
+    u_recv,
     p_send,
     p_recv,
     t_send,
@@ -109,14 +121,15 @@
 
     barrier = pltpu.get_barrier_semaphore()
     others = [device(z, x + r, core) for r in range(1, X_RING)]
-    others += [device(z + 1, x, core), device(z + Z_RING - 1, x, core), device(z, x, 1 - core)]
+    others += [device(z + k, x, core) for k in range(1, Z_RING)] + [device(z, x, 1 - core)]
     others += [{"tp": (tp + r) % tp_count} for r in range(1, tp_count)]
     for other in others:
         pl.semaphore_signal(barrier, inc=1, device_id=other, device_id_type=MESH)
     pl.semaphore_wait(barrier, len(others))
 
-    def slot(x_at):
-        return kv_ref.at[z, core, pl.ds(pl.multiple_of((x_at % X_RING) * tokens, tokens), tokens)]
+    def slot(x_at, z_at=z):
+        rows = pl.ds(pl.multiple_of((x_at % X_RING) * tokens, tokens), tokens)
+        return kv_ref.at[z_at % Z_RING, core, rows]
 
     def remote(src, dst, send_sem, recv_sem, to):
         return pltpu.make_async_remote_copy(
@@ -148,6 +161,28 @@
     def z_in(way, hop):
         return z_copy(way, hop, z + (Z_RING - 1 - hop if way == 0 else 1 + hop))
 
+    def v_copy(k, z_from):
+        return remote(
+            packed_ref, slot(x, z_from), v_send.at[k - 1], v_recv.at[k - 1], device(z + k, x, core)
+        )
+
+    def u_copy(k, r, x_from):
+        place = slot(x_from, z + Z_RING - k)
+        return remote(
+            place, place, u_send.at[k - 1, r - 1], u_recv.at[k - 1, r - 1], device(z, x + r, core)
+        )
+
+    def relay(distance):
+        for k in (distance, Z_RING - distance)[: 1 if 2 * distance == Z_RING else 2]:
+            v_copy(k, z + Z_RING - k).wait_recv()
+            for r in range(1, X_RING):
+                u_copy(k, r, x).start()
+
+    def relayed(distance):
+        for k in (distance, Z_RING - distance)[: 1 if 2 * distance == Z_RING else 2]:
+            for r in range(1, X_RING):
+                u_copy(k, r, x + X_RING - r).wait_recv()
+
     def p_copy(number, z_at, core_at):
         place = kv_ref.at[z_at % Z_RING, core_at]
         return remote(
@@ -162,6 +197,12 @@
     own.start()
     for r in range(1, X_RING):
         x_copy(r, x).start()
+
+    @pl.when(core == 1)
+    def _():
+        for k in (1, 7, 2, 6, 3, 5, 4):
+            v_copy(k, z).start()
+
     acc_ref[...] = jnp.zeros_like(acc_ref)
     sum_ref[...] = jnp.zeros_like(sum_ref)
     if guarded:
@@ -169,9 +210,16 @@
     own.wait()
     for r in range(1, X_RING):
         x_copy(r, x + X_RING - r).wait_recv()
-    z_out(0, 0).start()
-    z_out(1, 0).start()
     p_out(0).start()
+
+    @pl.when(core == 0)
+    def _():
+        z_out(0, 0).start()
+        z_out(1, 0).start()
+
+    @pl.when(core == 1)
+    def _():
+        relay(1)
 
     def step(j, carry):
         i = j + 2
@@ -181,17 +229,25 @@
 
         for hop in range(Z_RING // 2):
 
-            @pl.when(j == 4 * hop + 2)
+            @pl.when((j == 4 * hop + 2) & (core == 0))
             def _(hop=hop):
                 z_in(0, hop).wait_recv()
                 z_in(1, hop).wait_recv()
                 if hop < Z_RING // 2 - 1:
                     z_out(0, hop + 1).start()
                     z_out(1, hop + 1).start()
-                    p_out(2 * hop + 1).start()
+
+            @pl.when((j == 4 * hop + 2) & (core == 1))
+            def _(hop=hop):
+                if hop < Z_RING // 2 - 1:
+                    relay(hop + 2)
+                relayed(hop + 1)
+
+            @pl.when(j == 4 * hop + 2)
+            def _(hop=hop):
+                p_out(2 * hop + 1).start()
+                if hop < Z_RING // 2 - 1:
                     p_out(2 * hop + 2).start()
-                else:
-                    p_out(2 * hop + 1).start()
 
         @pl.when(member % 2 == 1)
         def _():
@@ -260,9 +316,20 @@
     own.wait()
     for r in range(1, X_RING):
         x_copy(r, x).wait_send()
-    for way in range(2):
-        for hop in range(Z_RING // 2):
-            z_out(way, hop).wait_send()
+
+    @pl.when(core == 0)
+    def _():
+        for way in range(2):
+            for hop in range(Z_RING // 2):
+                z_out(way, hop).wait_send()
+
+    @pl.when(core == 1)
+    def _():
+        for k in range(1, Z_RING):
+            v_copy(k, z).wait_send()
+            for r in range(1, X_RING):
+                u_copy(k, r, x).wait_send()
+
     for number in range(Z_RING):
         p_out(number).wait_send()
     for r in range(1, tp_count):
@@ -275,9 +342,8 @@
     out_proj_ref,
     residual_ref,
     ffn_gain_ref,
-    code_ref,
-    code_t_ref,
-    weight_ref,
+    routes_ref,
+    weights_ref,
     shared_gate_ref,
     shared_up_ref,
     shared_down_ref,
@@ -287,6 +353,8 @@
     out_ref,
     own_ref,
     hidden_ref,
+    rank_ref,
+    scale_ref,
     normed_ref,
     leaving_ref,
     passing_ref,
@@ -324,7 +392,8 @@
     tokens = part * tp_count
     quarter = width // 4
     rows = PLANE * 8
-    top = code_ref.shape[1]
+    top = routes_ref.shape[0]
+    experts = Z_RING * PLANE
 
     def at_z(z_at):
         return {"sp": (z_at % Z_RING) * PLANE + i}
@@ -363,6 +432,24 @@
             device_id_type=MESH,
         )
 
+    named = lax.broadcasted_iota(jnp.int32, (experts, tokens), 0) * tp_count + tp
+    hot = jnp.zeros((experts, tokens), jnp.float32)
+    scale = jnp.zeros((experts, tokens), jnp.float32)
+    for choice in range(top):
+        same = named == routes_ref[choice : choice + 1, :]
+        hot += jnp.where(same, 1.0, 0.0)
+        scale += jnp.where(same, weights_ref[choice : choice + 1, :], 0.0)
+    earlier = lax.broadcasted_iota(jnp.int32, (tokens, tokens), 0)
+    later = lax.broadcasted_iota(jnp.int32, (tokens, tokens), 1)
+    before = jnp.where(earlier < later, 1.0, 0.0).astype(jnp.bfloat16)
+    rank = jnp.dot(hot.astype(jnp.bfloat16), before, preferred_element_type=jnp.float32)
+    rank_ref[...] = jnp.where(hot > 0.0, rank, -1.0).reshape(Z_RING, PLANE, tokens)
+    scale_ref[...] = scale.reshape(Z_RING, PLANE, tokens)
+
+    def rows_of_eight(ref, z_at):
+        value = ref[z_at][:, None, :]
+        return jnp.broadcast_to(value, (PLANE, 8, tokens)).reshape(rows, tokens)
+
     loads[0].wait()
     size = heads_ref.shape[2]
     total = own_ref[...].astype(jnp.float32)
@@ -445,16 +532,10 @@
         k = turn(n)
         z_to = (z + k) % Z_RING
         row = lax.broadcasted_iota(jnp.int32, (rows, tokens), 0)
-        base = (z_to * PLANE + row // 8) * 16
-        main_code = base + row % 8
-        extra_code = base + 8 + (row % 8) // 4
-        main = jnp.zeros((rows, tokens), jnp.float32)
-        extra = jnp.zeros((rows, tokens), jnp.float32)
-        for slot in range(top):
-            own = code_t_ref[slot : slot + 1, :]
-            main += jnp.where(main_code == own, 1.0, 0.0)
-            extra += jnp.where(extra_code == own, 1.0, 0.0)
-        main = main.astype(jnp.bfloat16)
+        rank = rows_of_eight(rank_ref, z_to)
+        place = (row % 8).astype(jnp.float32)
+        main = jnp.where(rank == place, 1.0, 0.0).astype(jnp.bfloat16)
+        extra = jnp.where(rank == 8.0 + (row % 8 // 4).astype(jnp.float32), 1.0, 0.0)
         normed = normed_ref[...].reshape(tokens, width)
         tail = jnp.zeros((rows, quarter), jnp.float32)
         for q in range(4):
@@ -549,31 +630,28 @@
     def combine(z_at):
         tiles = back_ref[z_at].reshape(rows, width + quarter)
         twice = jnp.concatenate([tiles, tiles], axis=0)
-        lane = lax.broadcasted_iota(jnp.int32, (tokens, 2 * rows), 1)
-        place = lane % rows
-        base = (z_at * PLANE + place // 8) * 16
-        main_code = base + place % 8
-        extra_code = base + 8 + (place % 8) // 4
-        main = jnp.zeros((tokens, 2 * rows), jnp.float32)
-        extra = jnp.zeros((tokens, 2 * rows), jnp.float32)
-        for slot in range(top):
-            own = code_ref[:, slot : slot + 1]
-            scale = weight_ref[:, slot : slot + 1]
-            main += jnp.where(main_code == own, scale, 0.0)
-            extra += jnp.where(extra_code == own, scale, 0.0)
+        row = lax.broadcasted_iota(jnp.int32, (rows, tokens), 0)
+        rank = rows_of_eight(rank_ref, z_at)
+        scale = rows_of_eight(scale_ref, z_at)
+        place = (row % 8).astype(jnp.float32)
+        main = jnp.where(rank == place, scale, 0.0)
+        extra = jnp.where(rank == 8.0 + (row % 8 // 4).astype(jnp.float32), scale, 0.0)
 
         def two_terms(value):
-            high = value.astype(jnp.bfloat16).astype(jnp.float32)
-            return jnp.where(lane < rows, high, value - high)
-
-        main, extra = two_terms(main), two_terms(extra)
-        main = main.astype(jnp.bfloat16)
+            high = value.astype(jnp.bfloat16)
+            low = (value - high.astype(jnp.float32)).astype(jnp.bfloat16)
+            return jnp.concatenate([high, low], axis=0)
+
+        def product(terms, tiles):
+            return lax.dot_general(
+                terms, tiles, (((0,), (0,)), ((), ())), preferred_element_type=jnp.float32
+            )
+
+        main = two_terms(main)
         for q in range(4):
             cols = slice(q * quarter, (q + 1) * quarter)
-            chosen = jnp.where(place % 4 == q, extra, 0.0).astype(jnp.bfloat16)
-            acc_ref[:, cols] += jnp.dot(
-                main, twice[:, cols], preferred_element_type=jnp.float32
-            ) + jnp.dot(chosen, twice[:, width:], preferred_element_type=jnp.float32)
+            chosen = two_terms(jnp.where(row % 4 == q, extra, 0.0))
+            acc_ref[:, cols] += product(main, twice[:, cols]) + product(chosen, twice[:, width:])
 
     def returns(n, carry):
         @pl.when((n > 0) & (n < Z_RING))
@@ -647,21 +725,6 @@
 
 def shaped(dims, kind=jnp.bfloat16):
     return jax.ShapeDtypeStruct(dims, kind)
-
-
-def slot_codes(routes, tp_index, tp_count, sp_count):
-    tokens, top = routes.shape
-    flat = routes.reshape(-1)
-    is_mine = flat % tp_count == tp_index
-    target = flat // tp_count
-    onehot = (target[:, None] == jnp.arange(sp_count, dtype=jnp.int32)[None, :]) & is_mine[:, None]
-    hot = onehot.astype(jnp.bfloat16)
-    entries = tokens * top
-    order = jnp.arange(entries, dtype=jnp.int32)
-    before = (order[:, None] > order[None, :]).astype(jnp.bfloat16)
-    earlier = jnp.dot(before, hot, preferred_element_type=jnp.float32)
-    rank = jnp.sum(jnp.where(onehot, earlier, 0.0), axis=1).astype(jnp.int32)
-    return jnp.where(is_mine, target * 16 + rank, -1).reshape(tokens, top)
 
 
 def local(
@@ -687,25 +750,23 @@
     heads = queries.shape[1] // HEAD_SIZE
     sp_count = lax.axis_size("sp")
     tp_count = lax.axis_size("tp")
-    tp_index = lax.axis_index("tp")
     sequence_total = tokens * sp_count
     positions = lax.axis_index("sp") * tokens + jnp.arange(tokens, dtype=jnp.int32)
     cosine, sine = wide_tables(positions, sequence_total)
     columns = heads * tokens
-    query_rows, packed = call(
+    query_rows, packed, bound = call(
         prepare_kernel,
-        (shaped((columns, 128)), shaped((tokens, 128))),
+        (shaped((columns, 128)), shaped((tokens, 128)), shaped((8, 128), jnp.float32)),
         (
             queries,
-            jnp.concatenate([key_matrix, values], axis=1),
-            jnp.tile(query_gain, 2)[None],
-            jnp.tile(key_norm_gain, 2)[None],
+            key_matrix.T,
+            values.T,
+            query_gain[None],
+            key_norm_gain[None],
             cosine,
             sine,
         ),
     )
-    codes = slot_codes(routes, tp_index, tp_count, sp_count)
-    bound = 8.0 * jnp.max(jnp.abs(query_gain)) * jnp.max(jnp.abs(key_norm_gain))
     part_rows = tokens // tp_count
 
     def attention(guarded, number):
@@ -725,6 +786,10 @@
                     pltpu.SemaphoreType.DMA((X_RING - 1,)),
                     pltpu.SemaphoreType.DMA((2, Z_RING // 2)),
                     pltpu.SemaphoreType.DMA((2, Z_RING // 2)),
+                    pltpu.SemaphoreType.DMA((Z_RING - 1,)),
+                    pltpu.SemaphoreType.DMA((Z_RING - 1,)),
+                    pltpu.SemaphoreType.DMA((Z_RING - 1, X_RING - 1)),
+                    pltpu.SemaphoreType.DMA((Z_RING - 1, X_RING - 1)),
                     pltpu.SemaphoreType.DMA((Z_RING,)),
                     pltpu.SemaphoreType.DMA((Z_RING,)),
                     pltpu.SemaphoreType.DMA((tp_count - 1,)),
@@ -744,7 +809,7 @@
         return run
 
     tiles = lax.cond(
-        bound > SAFE_BOUND,
+        bound[0, 0] > SAFE_BOUND,
         attention(True, 1),
         attention(False, 0),
         query_rows,
@@ -759,11 +824,13 @@
     return pl.pallas_call(
         moe_kernel,
         out_shape=shaped((part_rows, width)),
-        in_specs=[VM, VM, ANY] + [VM] * 7 + [ANY] * 3,
+        in_specs=[VM, VM, ANY] + [VM] * 6 + [ANY] * 3,
         out_specs=VM,
         scratch_shapes=[
             pltpu.VMEM((part_rows, width), jnp.bfloat16),
             pltpu.VMEM((part_rows, width), jnp.float32),
+            pltpu.VMEM((Z_RING, PLANE, tokens), jnp.float32),
+            pltpu.VMEM((Z_RING, PLANE, tokens), jnp.float32),
             pltpu.VMEM((tp_count, part_rows, width), jnp.bfloat16),
             tile_set,
             tile_set,
@@ -802,9 +869,8 @@
         out_proj,
         residual,
         ffn_gain[None],
-        codes,
-        codes.T,
-        route_weights,
+        routes.T,
+        route_weights.T,
         shared_gate,
         shared_up,
         shared_down,

time: 256 us -> 248 us (0.969)
  the two profiles are of different devices: /device:TPU:161 before, /device:TPU:32 now
where the time goes in v4:
time: 248 us; the launch traced here: 247 us
  Pallas kernels  241 us (97%)
  local copies, waits for them, and re-layouts  2.99 us (1%)
    pallas_call x1, Pallas kernels, local(): pl.pallas_call(moe_kernel, out_shape=shaped((part_rows, width)), in_specs...  171 us
    pallas_call x1, Pallas kernels, run(): pl.pallas_call(functools.partial(ring_attention_kernel, guarded), out_sha...  68.4 us

profile of v4, /device:TPU:32, one launch (start us, length us, event | category | flops | bytes accessed | tf_op | source)
XLA Modules:
  0.0 247.1 jit_solution(7474533542923960915)
XLA Ops:
  0.0 0.1 mul.22
  0.1 1.9 sine_multiply_fusion
  2.1 2.2 shard_map.163
  4.2 1.2 slice.3
  6.1 68.6 %conditional.1 = (bf16[4,80,256]{2,1,0:T(8,128)(2,1)S(1)}) conditional(s32[]{:T(128)} %bitcast.4, (bf16[1280,128]{1,0:T(8,128)(2,1)S(1)}, bf16[320,128]{1,0:T(8,128)(2,1)S(1)}, f32[1,256]{1,0:T(1,128)}) %tuple.16, (bf16[1280,128]{1,0:T(8,128)(2,1)S(1)}, bf16[320,128]{1,0:T(8,128)(2,1)S(1)}, f32[1,256]{1,0:T(1,128)}) %tuple.17), branch_computations={%region_0.1_spmd, %region_1.2_spmd} | conditional | flops 13421772800 | bytes 5242888 | solution.py:811
  6.1 68.4 %branch_1_fun.1 = bf16[4,80,256]{2,1,0:T(8,128)(2,1)S(1)} custom-call(bf16[1280,128]{1,0:T(8,128)(2,1)S(1)} %get-tuple-element.23.q_ref, bf16[320,128]{1,0:T(8,128)(2,1)S(1)} %get-tuple-element.24.packed_ref, f32[1,256]{1,0:T(1,128)} %get-tuple-element.25.gain_ref), custom_call_target="tpu_custom_call" | custom-call | flops 13421772800 | bytes 5242880 | tf_op jit(solution)/shard_map/cond/branch_1_fun/pallas_call | solution.py:774
  74.7 170.7 %shard_map.164 = bf16[80,2048]{1,0:T(8,128)(2,1)} custom-call(bf16[4,80,256]{2,1,0:T(8,128)(2,1)S(1)} %get-tuple-element.36.heads_ref, bf16[1024,2048]{1,0:T(8,128)(2,1)} %out_proj_ref.1, bf16[320,2048]{1,0:T(8,128)(2,1)} %residual_ref.1, f32[1,2048]{1,0:T(1,128)} %bitcast.17, s32[4,320]{1,0:T(4,128)} %bitcast.18, f32[4,320]{1,0:T(4,128)} %bitcast.19, ...), custom_call_target="tpu_custom_call" | custom-call | tf_op jit(solution)/shard_map/pallas_call | solution.py:824
  245.4 1.7 copy.21
  (5 shorter events, 0.0 us)

commit v5 on v4

--- a/solution.py
+++ b/solution.py
@@ -23,18 +23,29 @@
     return field * lax.rsqrt(mean_sq + EPS) * gain
 
 
-def wide_tables(positions, sequence_total):
+def wide_tables(first, tokens, sequence_total):
     grid_rows = sequence_total // GRID_W
-    row_pos = (positions // GRID_W - grid_rows // 2).astype(jnp.float32)
-    col_pos = (positions % GRID_W - GRID_W // 2).astype(jnp.float32)
+    padded = -(-tokens // GRID_W // 8) * 8
+    row_pos = first // GRID_W + jnp.arange(padded, dtype=jnp.int32) - grid_rows // 2
+    col_pos = jnp.arange(GRID_W, dtype=jnp.int32) - GRID_W // 2
+    place = jnp.concatenate([row_pos, col_pos]).astype(jnp.float32)
     quarter = HEAD_SIZE // 4
     inverse = THETA ** (-jnp.arange(quarter, dtype=jnp.float32) / quarter)
     lane = jnp.arange(2 * HEAD_SIZE, dtype=jnp.int32)
-    inverse_wide = jnp.tile(inverse, 8)
-    is_row = (lane % HEAD_SIZE) < HEAD_SIZE // 2
-    angles = jnp.where(is_row[None, :], row_pos[:, None], col_pos[:, None]) * inverse_wide
+    angles = place[:, None] * jnp.tile(inverse, 8)
     sign = jnp.where((lane % 32) < 16, -1.0, 1.0)
     return jnp.cos(angles), jnp.sin(angles) * sign[None, :]
+
+
+def spread_table(table, tokens):
+    padded = table.shape[0] - GRID_W
+    count = tokens // GRID_W
+    by_row = jnp.concatenate(
+        [jnp.broadcast_to(table[n : n + 1], (GRID_W, 128)) for n in range(count)], axis=0
+    )
+    by_col = jnp.concatenate([table[padded:]] * count, axis=0)
+    lane = lax.broadcasted_iota(jnp.int32, (tokens, 128), 1)
+    return jnp.where(lane % HEAD_SIZE < HEAD_SIZE // 2, by_row, by_col)
 
 
 def normed_and_turned(field, gain, cosine, sine):
@@ -55,7 +66,8 @@
     q_ref, key_ref, value_ref, qg_ref, kg_ref, cos_ref, sin_ref, rows_ref, packed_ref, bound_ref
 ):
     tokens = q_ref.shape[0]
-    cosine, sine = cos_ref[...], sin_ref[...]
+    cosine = spread_table(cos_ref[...], tokens)
+    sine = spread_table(sin_ref[...], tokens)
     low = lax.broadcasted_iota(jnp.int32, (tokens, 128), 1) < HEAD_SIZE
     query_gain = jnp.concatenate([qg_ref[...], qg_ref[...]], axis=1)
     key_gain = jnp.concatenate([kg_ref[...], kg_ref[...]], axis=1)
@@ -464,102 +476,119 @@
     normed_ref[tp] = final_norm(hidden, ffn_gain_ref[...]).astype(jnp.bfloat16)
     pl.semaphore_wait(barrier, len(others))
 
-    def y_copy(r, source):
+    y_lanes = (pl.ds(0, quarter), pl.ds(quarter, width - quarter))
+    z_lanes = (pl.ds(0, quarter), pl.ds(quarter, width))
+    b_lanes = (pl.ds(0, width), pl.ds(width, quarter))
+    whole = pl.ds(0, width + quarter)
+
+    def y_copy(r, source, piece):
+        place = normed_ref.at[source % tp_count, :, y_lanes[piece]]
         return remote(
-            normed_ref.at[source % tp_count],
-            normed_ref.at[source % tp_count],
-            y_send.at[r - 1],
-            y_recv.at[r - 1],
-            at_tp(tp + r),
-        )
-
-    for r in (2, 1, 3):
-        y_copy(r, tp).start()
-    for r in range(1, tp_count):
-        y_copy(r, tp + tp_count - r).wait_recv()
+            place, place, y_send.at[r - 1, piece], y_recv.at[r - 1, piece], at_tp(tp + r)
+        )
+
+    for piece in range(2):
+        for r in (2, 1, 3):
+            y_copy(r, tp, piece).start()
 
     def turn(n):
         odd = n % 2
         return odd * ((n + 1) // 2) + (1 - odd) * ((Z_RING - n // 2) % Z_RING)
 
-    def z_copy(k, z_from, z_to):
+    def z_copy(k, z_from, z_to, piece):
         return remote(
-            leaving_ref.at[z_to % Z_RING],
-            passing_ref.at[z_from % Z_RING],
-            z_send.at[k],
-            z_recv.at[k],
+            leaving_ref.at[z_to % Z_RING, :, :, z_lanes[piece]],
+            passing_ref.at[z_from % Z_RING, :, :, z_lanes[piece]],
+            z_send.at[k, piece],
+            z_recv.at[k, piece],
             at_z(z + k),
         )
 
-    def bz_copy(k, z_from, z_to):
+    def bz_copy(k, z_from, z_to, piece):
         return remote(
-            made_ref.at[z_to % Z_RING],
-            back_passing_ref.at[z_from % Z_RING],
-            bz_send.at[k],
-            bz_recv.at[k],
+            made_ref.at[z_to % Z_RING, :, :, b_lanes[piece]],
+            back_passing_ref.at[z_from % Z_RING, :, :, b_lanes[piece]],
+            bz_send.at[k, piece],
+            bz_recv.at[k, piece],
             at_z(z + Z_RING - k),
         )
 
-    def i_copy(source_ref, target_ref, sends, recvs, k, z_at, r, tile, place):
+    out_way = (passing_ref, arrived_ref, i_send, i_recv, i_local, whole, 0)
+    back_ways = [
+        (back_passing_ref, back_ref, bi_send, bi_recv, bi_local, b_lanes[p], p * Z_RING)
+        for p in range(2)
+    ]
+
+    def i_copy(way, k, z_at, r, tile, place):
+        source_ref, target_ref, sends, recvs, _, lanes, shift = way
         return remote(
-            source_ref.at[z_at % Z_RING, tile % PLANE],
-            target_ref.at[z_at % Z_RING, place % PLANE],
-            sends.at[k, r - 1],
-            recvs.at[k, r - 1],
+            source_ref.at[z_at % Z_RING, tile % PLANE, :, lanes],
+            target_ref.at[z_at % Z_RING, place % PLANE, :, lanes],
+            sends.at[k + shift, r - 1],
+            recvs.at[k + shift, r - 1],
             at_i(i + r),
         )
 
-    def spread(source_ref, target_ref, sends, recvs, locals_, k, z_at):
+    def own_copy(way, k, z_at):
+        source_ref, target_ref, _, _, locals_, lanes, shift = way
+        return pltpu.make_async_copy(
+            source_ref.at[z_at % Z_RING, i, :, lanes],
+            target_ref.at[z_at % Z_RING, i, :, lanes],
+            locals_.at[k + shift],
+        )
+
+    def spread(way, k, z_at):
         for r in range(1, PLANE):
-            i_copy(source_ref, target_ref, sends, recvs, k, z_at, r, i + r, i).start()
-        pltpu.make_async_copy(
-            source_ref.at[z_at % Z_RING, i], target_ref.at[z_at % Z_RING, i], locals_.at[k]
-        ).start()
-
-    def collected(source_ref, target_ref, sends, recvs, locals_, k, z_at):
+            i_copy(way, k, z_at, r, i + r, i).start()
+        own_copy(way, k, z_at).start()
+
+    def collected(way, k, z_at):
         for r in range(1, PLANE):
-            place = i + PLANE - r
-            i_copy(source_ref, target_ref, sends, recvs, k, z_at, r, i, place).wait_recv()
-        pltpu.make_async_copy(
-            source_ref.at[z_at % Z_RING, i], target_ref.at[z_at % Z_RING, i], locals_.at[k]
-        ).wait()
-
-    def sent(source_ref, target_ref, sends, recvs, k, z_at):
+            i_copy(way, k, z_at, r, i, i + PLANE - r).wait_recv()
+        own_copy(way, k, z_at).wait()
+
+    def sent(way, k, z_at):
         for r in range(1, PLANE):
-            i_copy(source_ref, target_ref, sends, recvs, k, z_at, r, i + r, i).wait_send()
-
-    def dispatch(n, carry):
+            i_copy(way, k, z_at, r, i + r, i).wait_send()
+
+    def dispatch(piece, n, carry):
         k = turn(n)
         z_to = (z + k) % Z_RING
         row = lax.broadcasted_iota(jnp.int32, (rows, tokens), 0)
         rank = rows_of_eight(rank_ref, z_to)
         place = (row % 8).astype(jnp.float32)
         main = jnp.where(rank == place, 1.0, 0.0).astype(jnp.bfloat16)
-        extra = jnp.where(rank == 8.0 + (row % 8 // 4).astype(jnp.float32), 1.0, 0.0)
-        normed = normed_ref[...].reshape(tokens, width)
-        tail = jnp.zeros((rows, quarter), jnp.float32)
-        for q in range(4):
+        for q in range(1) if piece == 0 else range(1, 4):
             cols = slice(q * quarter, (q + 1) * quarter)
+            normed = normed_ref[:, :, cols].reshape(tokens, quarter)
             leaving_ref[z_to, :, :, cols] = (
-                jnp.dot(main, normed[:, cols], preferred_element_type=jnp.float32)
+                jnp.dot(main, normed, preferred_element_type=jnp.float32)
                 .astype(jnp.bfloat16)
                 .reshape(PLANE, 8, quarter)
             )
-            chosen = jnp.where(row % 4 == q, extra, 0.0).astype(jnp.bfloat16)
-            tail += jnp.dot(chosen, normed[:, cols], preferred_element_type=jnp.float32)
-        leaving_ref[z_to, :, :, width:] = tail.astype(jnp.bfloat16).reshape(PLANE, 8, quarter)
-
-        @pl.when(n == 0)
-        def _():
-            spread(leaving_ref, arrived_ref, i_send, i_recv, i_local, 0, z)
+        if piece == 1:
+            extra = jnp.where(rank == 8.0 + (row % 8 // 4).astype(jnp.float32), 1.0, 0.0)
+            tail = jnp.zeros((rows, quarter), jnp.float32)
+            for q in range(4):
+                normed = normed_ref[:, :, q * quarter : (q + 1) * quarter].reshape(tokens, quarter)
+                chosen = jnp.where(row % 4 == q, extra, 0.0).astype(jnp.bfloat16)
+                tail += jnp.dot(chosen, normed, preferred_element_type=jnp.float32)
+            leaving_ref[z_to, :, :, width:] = tail.astype(jnp.bfloat16).reshape(PLANE, 8, quarter)
+
+            @pl.when(n == 0)
+            def _():
+                spread((leaving_ref,) + out_way[1:], 0, z)
 
         @pl.when(n > 0)
         def _():
-            z_copy(k, z, z + k).start()
+            z_copy(k, z, z + k, piece).start()
 
         return carry
 
-    lax.fori_loop(0, Z_RING, dispatch, 0)
+    for piece in range(2):
+        for r in range(1, tp_count):
+            y_copy(r, tp + tp_count - r, piece).wait_recv()
+        lax.fori_loop(0, Z_RING, functools.partial(dispatch, piece), 0)
 
     normed = normed_ref[...].reshape(tokens, width)
     gate = jnp.dot(normed, shared_gate_ref[...], preferred_element_type=jnp.float32)
@@ -595,41 +624,49 @@
             made = jnp.dot(inner, down_ref[:, cols], preferred_element_type=jnp.float32).astype(
                 jnp.bfloat16
             )
-            made_ref[z_from, :, :, cols] = made[:rows].reshape(PLANE, 8, quarter)
+            made_ref[z_from, :, :, (q + 1) * quarter : (q + 2) * quarter] = made[:rows].reshape(
+                PLANE, 8, quarter
+            )
             pick = jnp.where(place == 4 * index + q, 1.0, 0.0).astype(jnp.bfloat16)
             tail += jnp.dot(pick, made[rows:], preferred_element_type=jnp.float32)
-        made_ref[z_from, :, :, width:] = tail.astype(jnp.bfloat16).reshape(PLANE, 8, quarter)
+        made_ref[z_from, :, :, :quarter] = tail.astype(jnp.bfloat16).reshape(PLANE, 8, quarter)
+
+    made_ways = [(made_ref,) + way[1:] for way in back_ways]
 
     def arrivals(n, carry):
         @pl.when((n > 0) & (n < Z_RING))
         def _():
             k = turn(n)
-            z_copy(k, z + Z_RING - k, z).wait_recv()
-            spread(passing_ref, arrived_ref, i_send, i_recv, i_local, k, z + Z_RING - k)
+            for piece in range(2):
+                z_copy(k, z + Z_RING - k, z, piece).wait_recv()
+            spread(out_way, k, z + Z_RING - k)
 
         @pl.when(n > 0)
         def _():
             k = turn(n - 1)
-            collected(
-                passing_ref, arrived_ref, i_send, i_recv, i_local, k, z + Z_RING - k
-            )
+            collected(out_way, k, z + Z_RING - k)
             expert(k)
 
             @pl.when(n > 1)
             def _():
-                bz_copy(k, z, z + Z_RING - k).start()
+                bz_copy(k, z, z + Z_RING - k, 0).start()
 
             @pl.when(n == 1)
             def _():
-                spread(made_ref, back_ref, bi_send, bi_recv, bi_local, 0, z)
+                spread(made_ways[0], 0, z)
 
         return carry
 
     lax.fori_loop(0, Z_RING + 1, arrivals, 0)
-
-    def combine(z_at):
-        tiles = back_ref[z_at].reshape(rows, width + quarter)
-        twice = jnp.concatenate([tiles, tiles], axis=0)
+    spread(made_ways[1], 0, z)
+    for k in (1, 7, 2, 6, 3, 5, 4):
+        bz_copy(k, z, z + Z_RING - k, 1).start()
+
+    def combine(piece, z_at):
+        def twice(start):
+            tiles = back_ref[z_at, :, :, start : start + quarter].reshape(rows, quarter)
+            return jnp.concatenate([tiles, tiles], axis=0)
+
         row = lax.broadcasted_iota(jnp.int32, (rows, tokens), 0)
         rank = rows_of_eight(rank_ref, z_at)
         scale = rows_of_eight(scale_ref, z_at)
@@ -650,62 +687,76 @@
         main = two_terms(main)
         for q in range(4):
             cols = slice(q * quarter, (q + 1) * quarter)
+            if piece == 1:
+                if q == 3:
+                    acc_ref[:, cols] += product(main, twice((q + 1) * quarter))
+                continue
             chosen = two_terms(jnp.where(row % 4 == q, extra, 0.0))
-            acc_ref[:, cols] += product(main, twice[:, cols]) + product(chosen, twice[:, width:])
-
-    def returns(n, carry):
+            added = product(chosen, twice(0))
+            if q < 3:
+                added += product(main, twice((q + 1) * quarter))
+            acc_ref[:, cols] += added
+
+    def returns(piece, n, carry):
         @pl.when((n > 0) & (n < Z_RING))
         def _():
             k = turn(n)
-            bz_copy(k, z + k, z).wait_recv()
-            spread(back_passing_ref, back_ref, bi_send, bi_recv, bi_local, k, z + k)
+            bz_copy(k, z + k, z, piece).wait_recv()
+            spread(back_ways[piece], k, z + k)
 
         @pl.when(n > 0)
         def _():
             k = turn(n - 1)
-            collected(back_passing_ref, back_ref, bi_send, bi_recv, bi_local, k, z + k)
-            combine((z + k) % Z_RING)
+            collected(back_ways[piece], k, z + k)
+            combine(piece, (z + k) % Z_RING)
 
         return carry
 
-    lax.fori_loop(0, Z_RING + 1, returns, 0)
-
-    def s_copy(r, source):
+    s_lanes = (pl.ds(0, 3 * quarter), pl.ds(3 * quarter, quarter))
+
+    def s_copy(r, source, piece):
         return remote(
-            part_ref.at[(tp + r) % tp_count],
-            got_ref.at[source % tp_count],
-            s_send.at[r - 1],
-            s_recv.at[r - 1],
+            part_ref.at[(tp + r) % tp_count, :, s_lanes[piece]],
+            got_ref.at[source % tp_count, :, s_lanes[piece]],
+            s_send.at[r - 1, piece],
+            s_recv.at[r - 1, piece],
             at_tp(tp + r),
         )
 
-    for r in (2, 1, 3, 0):
-        owner = (tp + r) % tp_count
-        own_rows = pl.ds(pl.multiple_of(owner * part, part), part)
-        part_ref[owner] = acc_ref[own_rows, :].astype(jnp.bfloat16)
-        if r:
-            s_copy(r, tp).start()
-        else:
-            got_ref[tp] = part_ref[tp]
-    for r in range(1, tp_count):
-        s_copy(r, tp + tp_count - r).wait_recv()
+    for piece in range(2):
+        lax.fori_loop(0, Z_RING + 1, functools.partial(returns, piece), 0)
+        for r in (2, 1, 3, 0):
+            owner = (tp + r) % tp_count
+            own_rows = pl.ds(pl.multiple_of(owner * part, part), part)
+            lanes = s_lanes[piece]
+            part_ref[owner, :, lanes] = acc_ref[own_rows, lanes].astype(jnp.bfloat16)
+            if r:
+                s_copy(r, tp, piece).start()
+            else:
+                got_ref[tp, :, lanes] = part_ref[tp, :, lanes]
+    for piece in range(2):
+        for r in range(1, tp_count):
+            s_copy(r, tp + tp_count - r, piece).wait_recv()
     total = hidden_ref[...]
     for t in range(tp_count):
         total += got_ref[t].astype(jnp.float32)
     out_ref[...] = total.astype(jnp.bfloat16)
 
-    for r in range(1, tp_count):
-        y_copy(r, tp).wait_send()
-        s_copy(r, tp).wait_send()
+    for piece in range(2):
+        for r in range(1, tp_count):
+            y_copy(r, tp, piece).wait_send()
+            s_copy(r, tp, piece).wait_send()
 
     def drain(n, carry):
         @pl.when(n > 0)
         def _():
-            z_copy(n, z, z + n).wait_send()
-            bz_copy(n, z, z + Z_RING - n).wait_send()
-
-        sent(passing_ref, arrived_ref, i_send, i_recv, n, z + Z_RING - n)
-        sent(back_passing_ref, back_ref, bi_send, bi_recv, n, z + n)
+            for piece in range(2):
+                z_copy(n, z, z + n, piece).wait_send()
+                bz_copy(n, z, z + Z_RING - n, piece).wait_send()
+
+        sent(out_way, n, z + Z_RING - n)
+        for piece in range(2):
+            sent(back_ways[piece], n, z + n)
         return carry
 
     lax.fori_loop(0, Z_RING, drain, 0)
@@ -751,8 +802,7 @@
     sp_count = lax.axis_size("sp")
     tp_count = lax.axis_size("tp")
     sequence_total = tokens * sp_count
-    positions = lax.axis_index("sp") * tokens + jnp.arange(tokens, dtype=jnp.int32)
-    cosine, sine = wide_tables(positions, sequence_total)
+    cosine, sine = wide_tables(lax.axis_index("sp") * tokens, tokens, sequence_total)
     columns = heads * tokens
     query_rows, packed, bound = call(
         prepare_kernel,
@@ -846,20 +896,20 @@
             pltpu.VMEM((hidden_units, width), jnp.bfloat16),
             dma((3,)),
             dma,
-            dma((tp_count - 1,)),
-            dma((tp_count - 1,)),
-            dma((tp_count - 1,)),
-            dma((tp_count - 1,)),
-            dma((Z_RING,)),
-            dma((Z_RING,)),
+            dma((tp_count - 1, 2)),
+            dma((tp_count - 1, 2)),
+            dma((tp_count - 1, 2)),
+            dma((tp_count - 1, 2)),
+            dma((Z_RING, 2)),
+            dma((Z_RING, 2)),
             dma((Z_RING, PLANE - 1)),
             dma((Z_RING, PLANE - 1)),
             dma((Z_RING,)),
-            dma((Z_RING,)),
-            dma((Z_RING,)),
-            dma((Z_RING, PLANE - 1)),
-            dma((Z_RING, PLANE - 1)),
-            dma((Z_RING,)),
+            dma((Z_RING, 2)),
+            dma((Z_RING, 2)),
+            dma((2 * Z_RING, PLANE - 1)),
+            dma((2 * Z_RING, PLANE - 1)),
+            dma((2 * Z_RING,)),
         ],
         compiler_params=pltpu.CompilerParams(
             vmem_limit_bytes=58 * 2**20, collective_id=2, has_side_effects=True

time: 248 us -> 232 us (0.935)
  Pallas kernels: 241 us -> 227 us
    pallas_call x1, Pallas kernels: 171 us -> 157 us  [local(): pl.pallas_call(moe_kernel, out_shape=shaped((part_rows, width)), in_specs...]
where the time goes in v5:
time: 232 us
  Pallas kernels  227 us (98%)
  local copies, waits for them, and re-layouts  2.98 us (1%)
    pallas_call x1, Pallas kernels, local(): pl.pallas_call(moe_kernel, out_shape=shaped((part_rows, width)), in_specs...  157 us
    pallas_call x1, Pallas kernels, run(): pl.pallas_call(functools.partial(ring_attention_kernel, guarded), out_sha...  68.4 us

profile of v5, /device:TPU:32, one launch (start us, length us, event | category | flops | bytes accessed | tf_op | source)
XLA Modules:
  0.0 231.9 jit_solution(2105092757507410494)
XLA Ops:
  0.0 0.1 add_convert_fusion
  0.1 0.1 mul.28
  0.2 0.8 fusion
  1.0 2.0 shard_map.163
  3.1 1.2 slice.3
  4.9 68.6 %conditional.1 = (bf16[4,80,256]{2,1,0:T(8,128)(2,1)S(1)}) conditional(s32[]{:T(128)} %bitcast.4, (bf16[1280,128]{1,0:T(8,128)(2,1)S(1)}, bf16[320,128]{1,0:T(8,128)(2,1)S(1)}, f32[1,256]{1,0:T(1,128)}) %tuple.15, (bf16[1280,128]{1,0:T(8,128)(2,1)S(1)}, bf16[320,128]{1,0:T(8,128)(2,1)S(1)}, f32[1,256]{1,0:T(1,128)}) %tuple.16), branch_computations={%region_0.1_spmd, %region_1.2_spmd} | conditional | flops 13421772800 | bytes 5242888 | solution.py:861
  4.9 68.4 %branch_1_fun.1 = bf16[4,80,256]{2,1,0:T(8,128)(2,1)S(1)} custom-call(bf16[1280,128]{1,0:T(8,128)(2,1)S(1)} %get-tuple-element.23.q_ref, bf16[320,128]{1,0:T(8,128)(2,1)S(1)} %get-tuple-element.24.packed_ref, f32[1,256]{1,0:T(1,128)} %get-tuple-element.25.gain_ref), custom_call_target="tpu_custom_call" | custom-call | flops 13421772800 | bytes 5242880 | tf_op jit(solution)/shard_map/cond/branch_1_fun/pallas_call | solution.py:824
  73.5 156.7 %shard_map.164 = bf16[80,2048]{1,0:T(8,128)(2,1)} custom-call(bf16[4,80,256]{2,1,0:T(8,128)(2,1)S(1)} %get-tuple-element.34.heads_ref, bf16[1024,2048]{1,0:T(8,128)(2,1)} %out_proj_ref.1, bf16[320,2048]{1,0:T(8,128)(2,1)} %residual_ref.1, f32[1,2048]{1,0:T(1,128)} %bitcast.17, s32[4,320]{1,0:T(4,128)} %bitcast.18, f32[4,320]{1,0:T(4,128)} %bitcast.19, ...), custom_call_target="tpu_custom_call" | custom-call | tf_op jit(solution)/shard_map/pallas_call | solution.py:874
  230.2 1.7 copy.21
  (5 shorter events, 0.0 us)

commit v6 on v5

--- a/solution.py
+++ b/solution.py
@@ -73,7 +73,7 @@
     key_gain = jnp.concatenate([kg_ref[...], kg_ref[...]], axis=1)
     top = jnp.max(jnp.abs(query_gain), axis=1, keepdims=True)
     top = top * jnp.max(jnp.abs(key_gain), axis=1, keepdims=True) * (HEAD_SIZE**0.5)
-    bound_ref[...] = jnp.broadcast_to(top, bound_ref.shape)
+    bound_ref[0, 0] = jnp.max(jnp.broadcast_to(top, (8, 128)))
     both = jnp.concatenate(
         [key_ref[...].astype(jnp.float32), value_ref[...].astype(jnp.float32)], axis=0
     ).T
@@ -94,7 +94,7 @@
 PLANE = 2 * X_RING
 
 
-def ring_attention_kernel(
+def ring_attention(
     guarded,
     q_ref,
     packed_ref,
@@ -131,14 +131,6 @@
     def device(z_at, x_at, core_at):
         return {"sp": ((z_at % Z_RING) * X_RING + x_at % X_RING) * 2 + core_at}
 
-    barrier = pltpu.get_barrier_semaphore()
-    others = [device(z, x + r, core) for r in range(1, X_RING)]
-    others += [device(z + k, x, core) for k in range(1, Z_RING)] + [device(z, x, 1 - core)]
-    others += [{"tp": (tp + r) % tp_count} for r in range(1, tp_count)]
-    for other in others:
-        pl.semaphore_signal(barrier, inc=1, device_id=other, device_id_type=MESH)
-    pl.semaphore_wait(barrier, len(others))
-
     def slot(x_at, z_at=z):
         rows = pl.ds(pl.multiple_of((x_at % X_RING) * tokens, tokens), tokens)
         return kv_ref.at[z_at % Z_RING, core, rows]
@@ -349,20 +341,29 @@
         t_copy(r, tp).wait_send()
 
 
-def moe_kernel(
-    heads_ref,
-    out_proj_ref,
+def layer_kernel(
+    guarded,
+    q_ref,
+    packed_ref,
+    gain_ref,
     residual_ref,
     ffn_gain_ref,
     routes_ref,
     weights_ref,
-    shared_gate_ref,
-    shared_up_ref,
-    shared_down_ref,
+    out_proj_hbm,
+    shared_gate_hbm,
+    shared_up_hbm,
+    shared_down_hbm,
     gate_hbm,
     up_hbm,
     down_hbm,
     out_ref,
+    attention_scratch,
+    heads_ref,
+    out_proj_ref,
+    shared_gate_ref,
+    shared_up_ref,
+    shared_down_ref,
     own_ref,
     hidden_ref,
     rank_ref,
@@ -427,10 +428,18 @@
         pltpu.make_async_copy(
             residual_ref.at[pl.ds(pl.multiple_of(tp * part, part), part)], own_ref, l_sem
         ),
-        pltpu.make_async_copy(gate_hbm, gate_ref, w_sem.at[0]),
-        pltpu.make_async_copy(up_hbm, up_ref, w_sem.at[1]),
-        pltpu.make_async_copy(down_hbm, down_ref, w_sem.at[2]),
     ]
+    weights = (
+        (out_proj_hbm, out_proj_ref),
+        (shared_gate_hbm, shared_gate_ref),
+        (shared_up_hbm, shared_up_ref),
+        (shared_down_hbm, shared_down_ref),
+        (gate_hbm, gate_ref),
+        (up_hbm, up_ref),
+        (down_hbm, down_ref),
+    )
+    for number, (source, target) in enumerate(weights):
+        loads.append(pltpu.make_async_copy(source, target, w_sem.at[number]))
     for load in loads:
         load.start()
 
@@ -462,7 +471,11 @@
         value = ref[z_at][:, None, :]
         return jnp.broadcast_to(value, (PLANE, 8, tokens)).reshape(rows, tokens)
 
-    loads[0].wait()
+    pl.semaphore_wait(barrier, len(others))
+    ring_attention(guarded, q_ref, packed_ref, gain_ref, heads_ref, *attention_scratch)
+
+    for load in loads:
+        load.wait()
     size = heads_ref.shape[2]
     total = own_ref[...].astype(jnp.float32)
     for t in range(tp_count):
@@ -474,8 +487,6 @@
     hidden = total.astype(jnp.bfloat16).astype(jnp.float32)
     hidden_ref[...] = hidden
     normed_ref[tp] = final_norm(hidden, ffn_gain_ref[...]).astype(jnp.bfloat16)
-    pl.semaphore_wait(barrier, len(others))
-
     y_lanes = (pl.ds(0, quarter), pl.ds(quarter, width - quarter))
     z_lanes = (pl.ds(0, quarter), pl.ds(quarter, width))
     b_lanes = (pl.ds(0, width), pl.ds(width, quarter))
@@ -595,8 +606,6 @@
     up = jnp.dot(normed, shared_up_ref[...], preferred_element_type=jnp.float32)
     inner = (gate / (1.0 + jnp.exp(-gate)) * up).astype(jnp.bfloat16)
     acc_ref[...] = jnp.dot(inner, shared_down_ref[...], preferred_element_type=jnp.float32)
-    for load in loads[1:]:
-        load.wait()
 
     def expert(k):
         z_from = (z + Z_RING - k) % Z_RING
@@ -762,15 +771,12 @@
     lax.fori_loop(0, Z_RING, drain, 0)
 
 
-def call(kernel, out_shape, args, specs=None, scratch=(), flops=0, moved=0):
+def call(kernel, out_shape, out_specs, args):
     return pl.pallas_call(
         kernel,
         out_shape=out_shape,
-        in_specs=specs or [VM] * len(args),
-        out_specs=jax.tree.map(lambda _: VM, out_shape),
-        scratch_shapes=scratch,
-        compiler_params=pltpu.CompilerParams(vmem_limit_bytes=56 * 2**20),
-        cost_estimate=pl.CostEstimate(flops=flops, bytes_accessed=moved, transcendentals=0),
+        in_specs=[VM] * len(args),
+        out_specs=out_specs,
     )(*args)
 
 
@@ -806,7 +812,8 @@
     columns = heads * tokens
     query_rows, packed, bound = call(
         prepare_kernel,
-        (shaped((columns, 128)), shaped((tokens, 128)), shaped((8, 128), jnp.float32)),
+        (shaped((columns, 128)), shaped((tokens, 128)), shaped((1, 1), jnp.float32)),
+        (VM, VM, pl.BlockSpec(memory_space=pltpu.SMEM)),
         (
             queries,
             key_matrix.T,
@@ -819,108 +826,24 @@
     )
     part_rows = tokens // tp_count
 
-    def attention(guarded, number):
-        def run(rows, own, gain):
-            return pl.pallas_call(
-                functools.partial(ring_attention_kernel, guarded),
-                out_shape=shaped((tp_count, part_rows, heads * HEAD_SIZE)),
-                in_specs=[VM, VM, VM],
-                out_specs=VM,
-                scratch_shapes=[
-                    pltpu.VMEM((Z_RING, 2, X_RING * tokens, 128), jnp.bfloat16),
-                    pltpu.VMEM((tokens, heads * HEAD_SIZE), jnp.bfloat16),
-                    pltpu.VMEM((HEAD_SIZE, columns), jnp.float32),
-                    pltpu.VMEM((8, columns), jnp.float32),
-                    pltpu.VMEM((1, columns), jnp.float32),
-                    pltpu.SemaphoreType.DMA((X_RING - 1,)),
-                    pltpu.SemaphoreType.DMA((X_RING - 1,)),
-                    pltpu.SemaphoreType.DMA((2, Z_RING // 2)),
-                    pltpu.SemaphoreType.DMA((2, Z_RING // 2)),
-                    pltpu.SemaphoreType.DMA((Z_RING - 1,)),
-                    pltpu.SemaphoreType.DMA((Z_RING - 1,)),
-                    pltpu.SemaphoreType.DMA((Z_RING - 1, X_RING - 1)),
-                    pltpu.SemaphoreType.DMA((Z_RING - 1, X_RING - 1)),
-                    pltpu.SemaphoreType.DMA((Z_RING,)),
-                    pltpu.SemaphoreType.DMA((Z_RING,)),
-                    pltpu.SemaphoreType.DMA((tp_count - 1,)),
-                    pltpu.SemaphoreType.DMA((tp_count - 1,)),
-                    pltpu.SemaphoreType.DMA,
-                ],
-                compiler_params=pltpu.CompilerParams(
-                    vmem_limit_bytes=56 * 2**20, collective_id=number, has_side_effects=True
-                ),
-                cost_estimate=pl.CostEstimate(
-                    flops=4 * columns * sequence_total * 128,
-                    bytes_accessed=sequence_total * 256,
-                    transcendentals=0,
-                ),
-            )(rows, own, gain)
-
-        return run
-
-    tiles = lax.cond(
-        bound[0, 0] > SAFE_BOUND,
-        attention(True, 1),
-        attention(False, 0),
-        query_rows,
-        packed,
-        head_gain[None],
-    )
     width = residual.shape[1]
     hidden_units = expert_gate.shape[2]
     wide_row = width + width // 4
     tile_set = pltpu.VMEM((Z_RING, PLANE, 8, wide_row), jnp.bfloat16)
     dma = pltpu.SemaphoreType.DMA
-    return pl.pallas_call(
-        moe_kernel,
-        out_shape=shaped((part_rows, width)),
-        in_specs=[VM, VM, ANY] + [VM] * 6 + [ANY] * 3,
-        out_specs=VM,
-        scratch_shapes=[
-            pltpu.VMEM((part_rows, width), jnp.bfloat16),
-            pltpu.VMEM((part_rows, width), jnp.float32),
-            pltpu.VMEM((Z_RING, PLANE, tokens), jnp.float32),
-            pltpu.VMEM((Z_RING, PLANE, tokens), jnp.float32),
-            pltpu.VMEM((tp_count, part_rows, width), jnp.bfloat16),
-            tile_set,
-            tile_set,
-            tile_set,
-            tile_set,
-            tile_set,
-            tile_set,
-            pltpu.VMEM((tokens, width), jnp.float32),
-            pltpu.VMEM((tp_count, part_rows, width), jnp.bfloat16),
-            pltpu.VMEM((tp_count, part_rows, width), jnp.bfloat16),
-            pltpu.VMEM((width, hidden_units), jnp.bfloat16),
-            pltpu.VMEM((width, hidden_units), jnp.bfloat16),
-            pltpu.VMEM((hidden_units, width), jnp.bfloat16),
-            dma((3,)),
-            dma,
-            dma((tp_count - 1, 2)),
-            dma((tp_count - 1, 2)),
-            dma((tp_count - 1, 2)),
-            dma((tp_count - 1, 2)),
-            dma((Z_RING, 2)),
-            dma((Z_RING, 2)),
-            dma((Z_RING, PLANE - 1)),
-            dma((Z_RING, PLANE - 1)),
-            dma((Z_RING,)),
-            dma((Z_RING, 2)),
-            dma((Z_RING, 2)),
-            dma((2 * Z_RING, PLANE - 1)),
-            dma((2 * Z_RING, PLANE - 1)),
-            dma((2 * Z_RING,)),
-        ],
-        compiler_params=pltpu.CompilerParams(
-            vmem_limit_bytes=58 * 2**20, collective_id=2, has_side_effects=True
-        ),
-    )(
-        tiles,
-        out_proj,
+
+    def like(weight):
+        return pltpu.VMEM(weight.shape, weight.dtype)
+
+    operands = (
+        query_rows,
+        packed,
+        head_gain[None],
         residual,
         ffn_gain[None],
         routes.T,
         route_weights.T,
+        out_proj,
         shared_gate,
         shared_up,
         shared_down,
@@ -928,6 +851,80 @@
         expert_up[0],
         expert_down[0],
     )
+    attention_scratch = (
+        pltpu.VMEM((Z_RING, 2, X_RING * tokens, 128), jnp.bfloat16),
+        pltpu.VMEM((tokens, heads * HEAD_SIZE), jnp.bfloat16),
+        pltpu.VMEM((HEAD_SIZE, columns), jnp.float32),
+        pltpu.VMEM((8, columns), jnp.float32),
+        pltpu.VMEM((1, columns), jnp.float32),
+        dma((X_RING - 1,)),
+        dma((X_RING - 1,)),
+        dma((2, Z_RING // 2)),
+        dma((2, Z_RING // 2)),
+        dma((Z_RING - 1,)),
+        dma((Z_RING - 1,)),
+        dma((Z_RING - 1, X_RING - 1)),
+        dma((Z_RING - 1, X_RING - 1)),
+        dma((Z_RING,)),
+        dma((Z_RING,)),
+        dma((tp_count - 1,)),
+        dma((tp_count - 1,)),
+        dma,
+    )
+
+    def layer(guarded, number):
+        return pl.pallas_call(
+            functools.partial(layer_kernel, guarded),
+            out_shape=shaped((part_rows, width)),
+            in_specs=[VM] * 3 + [ANY] + [VM] * 3 + [ANY] * 7,
+            out_specs=VM,
+            scratch_shapes=[
+                attention_scratch,
+                pltpu.VMEM((tp_count, part_rows, heads * HEAD_SIZE), jnp.bfloat16),
+                like(out_proj),
+                like(shared_gate),
+                like(shared_up),
+                like(shared_down),
+                pltpu.VMEM((part_rows, width), jnp.bfloat16),
+                pltpu.VMEM((part_rows, width), jnp.float32),
+                pltpu.VMEM((Z_RING, PLANE, tokens), jnp.float32),
+                pltpu.VMEM((Z_RING, PLANE, tokens), jnp.float32),
+                pltpu.VMEM((tp_count, part_rows, width), jnp.bfloat16),
+                tile_set,
+                tile_set,
+                tile_set,
+                tile_set,
+                tile_set,
+                tile_set,
+                pltpu.VMEM((tokens, width), jnp.float32),
+                pltpu.VMEM((tp_count, part_rows, width), jnp.bfloat16),
+                pltpu.VMEM((tp_count, part_rows, width), jnp.bfloat16),
+                like(expert_gate[0]),
+                like(expert_up[0]),
+                like(expert_down[0]),
+                dma((7,)),
+                dma,
+                dma((tp_count - 1, 2)),
+                dma((tp_count - 1, 2)),
+                dma((tp_count - 1, 2)),
+                dma((tp_count - 1, 2)),
+                dma((Z_RING, 2)),
+                dma((Z_RING, 2)),
+                dma((Z_RING, PLANE - 1)),
+                dma((Z_RING, PLANE - 1)),
+                dma((Z_RING,)),
+                dma((Z_RING, 2)),
+                dma((Z_RING, 2)),
+                dma((2 * Z_RING, PLANE - 1)),
+                dma((2 * Z_RING, PLANE - 1)),
+                dma((2 * Z_RING,)),
+            ],
+            compiler_params=pltpu.CompilerParams(
+                vmem_limit_bytes=62 * 2**20, collective_id=number, has_side_effects=True
+            ),
+        )
+
+    return lax.cond(bound[0, 0] > SAFE_BOUND, layer(True, 1), layer(False, 0), *operands)
 
 
 def solution(mesh):

time: 232 us -> 223 us (0.961)
  Pallas kernels: 227 us -> 221 us
    pallas_call x3 -> x2, Pallas kernels: 227 us -> 221 us  [the longest x1 219 us: local(): lax.cond(bound[0, 0] > SAFE_BOUND, layer(True, 1), layer(False, 0), *oper...]
where the time goes in v6:
time: 223 us
  Pallas kernels  221 us (99%)
    pallas_call x1, Pallas kernels, local(): lax.cond(bound[0, 0] > SAFE_BOUND, layer(True, 1), layer(False, 0), *oper...  219 us

profile of v6, /device:TPU:32, one launch (start us, length us, event | category | flops | bytes accessed | tf_op | source)
XLA Modules:
  0.0 223.3 jit_solution(3935565741705617536)
XLA Ops:
  0.0 0.1 add_convert_fusion
  0.1 0.1 mul.28
  0.2 0.8 fusion
  1.0 2.0 shard_map.165
  3.6 218.9 %conditional.1 = (bf16[80,2048]{1,0:T(8,128)(2,1)S(1)}) conditional(s32[]{:T(128)} %bitcast.4, (bf16[1280,128]{1,0:T(8,128)(2,1)S(1)}, bf16[320,128]{1,0:T(8,128)(2,1)S(1)}, f32[1,256]{1,0:T(1,128)}, bf16[320,2048]{1,0:T(8,128)(2,1)}, f32[1,2048]{1,0:T(1,128)}, /*index=5*/s32[4,320]{1,0:T(4,128)}, f32[4,320]{1,0:T(4,128)}, ...), branch_computations={%region_0.1_spmd, %region_1.2_spmd} | conditional | bytes 8 | solution.py:927
  3.8 218.7 %branch_1_fun.1 = bf16[80,2048]{1,0:T(8,128)(2,1)S(1)} custom-call(bf16[1280,128]{1,0:T(8,128)(2,1)S(1)} %get-tuple-element.78.q_ref, bf16[320,128]{1,0:T(8,128)(2,1)S(1)} %get-tuple-element.79.packed_ref, f32[1,256]{1,0:T(1,128)} %get-tuple-element.80.gain_ref, bf16[320,2048]{1,0:T(8,128)(2,1)} %get-tuple-element.81.residual_ref, ...), custom_call_target="tpu_custom_call" | custom-call | tf_op jit(solution)/shard_map/cond/branch_1_fun/pallas_call | solution.py:927
  222.6 0.7 copy.23
  (5 shorter events, 0.0 us)

commit v7 on v6

--- a/solution.py
+++ b/solution.py
@@ -504,7 +504,8 @@
 
     def turn(n):
         odd = n % 2
-        return odd * ((n + 1) // 2) + (1 - odd) * ((Z_RING - n // 2) % Z_RING)
+        even = (Z_RING // 2 + n // 2) * ((n + Z_RING - 1) // Z_RING)
+        return odd * ((Z_RING + 1 - n) // 2) + (1 - odd) * even
 
     def z_copy(k, z_from, z_to, piece):
         return remote(
@@ -668,7 +669,7 @@
 
     lax.fori_loop(0, Z_RING + 1, arrivals, 0)
     spread(made_ways[1], 0, z)
-    for k in (1, 7, 2, 6, 3, 5, 4):
+    for k in (4, 5, 3, 6, 2, 7, 1):
         bz_copy(k, z, z + Z_RING - k, 1).start()
 
     def combine(piece, z_at):

time: 223 us -> 222 us (level); the launches traced: 223 us -> 219 us
  Pallas kernels: 221 us -> 216 us
    pallas_call x1, Pallas kernels: 219 us -> 214 us  [local(): lax.cond(bound[0, 0] > SAFE_BOUND, layer(True, 1), layer(False, 0), *oper...]
where the time goes in v7:
time: 222 us; the launch traced here: 219 us
  Pallas kernels  216 us (97%)
    pallas_call x1, Pallas kernels, local(): lax.cond(bound[0, 0] > SAFE_BOUND, layer(True, 1), layer(False, 0), *oper...  214 us

profile of v7, /device:TPU:32, one launch (start us, length us, event | category | flops | bytes accessed | tf_op | source)
XLA Modules:
  0.0 219.0 jit_solution(11534658888615556552)
XLA Ops:
  0.0 0.1 add_convert_fusion
  0.1 0.1 mul.28
  0.2 0.8 fusion
  1.0 2.0 shard_map.165
  3.6 214.6 %conditional.1 = (bf16[80,2048]{1,0:T(8,128)(2,1)S(1)}) conditional(s32[]{:T(128)} %bitcast.4, (bf16[1280,128]{1,0:T(8,128)(2,1)S(1)}, bf16[320,128]{1,0:T(8,128)(2,1)S(1)}, f32[1,256]{1,0:T(1,128)}, bf16[320,2048]{1,0:T(8,128)(2,1)}, f32[1,2048]{1,0:T(1,128)}, /*index=5*/s32[4,320]{1,0:T(4,128)}, f32[4,320]{1,0:T(4,128)}, ...), branch_computations={%region_0.1_spmd, %region_1.2_spmd} | conditional | bytes 8 | solution.py:928
  3.8 214.4 %branch_1_fun.1 = bf16[80,2048]{1,0:T(8,128)(2,1)S(1)} custom-call(bf16[1280,128]{1,0:T(8,128)(2,1)S(1)} %get-tuple-element.78.q_ref, bf16[320,128]{1,0:T(8,128)(2,1)S(1)} %get-tuple-element.79.packed_ref, f32[1,256]{1,0:T(1,128)} %get-tuple-element.80.gain_ref, bf16[320,2048]{1,0:T(8,128)(2,1)} %get-tuple-element.81.residual_ref, ...), custom_call_target="tpu_custom_call" | custom-call | tf_op jit(solution)/shard_map/cond/branch_1_fun/pallas_call | solution.py:928
  218.2 0.7 copy.23
  (5 shorter events, 0.0 us)
